TPU v7x, 256 devices: a whole 4x4x8 slice. The times are simulated.
256 devices in a mesh: sp: 16 (over y, x), dp: 16 (over z, core).
Axes of the slice: x: 4, y: 4, z: 8, core: 2. Of those that a mesh axis runs over, the one named last changes fastest.
Arguments:
- tokens: bfloat16 [16, 3072, 4096], P('dp', 'sp'), may hold values from -30 to 30
- query_weight: bfloat16 [4096, 2048], P('dp', 'sp'), may hold values from -0.09375 to 0.09375
- key_weight: bfloat16 [4096, 2048], P('dp', 'sp'), may hold values from -0.09375 to 0.09375
- value_weight: bfloat16 [4096, 2048], P('dp', 'sp'), may hold values from -0.09375 to 0.09375
- cum_gate: float32 [16, 16, 3072], P('dp', 'sp'), may hold values from -12288 to 0, as said below
Outputs:
- attended: bfloat16 [16, 3072, 2048], P('dp', 'sp')
Inputs may be any that keep to these rules, and one draw needn't show every extreme that they name: `cum_gate`: never rising along positions; the first position holds one step's log gate.
All inputs are finite; a program needn't handle non-finite values.
Results may differ from a plain program's by a relative error of at most 0.0076.
The roundings to bfloat16 on the way count: a program that leaves them out, or rounds other values in their place, can miss the bound.
Values may be sent and summed in bfloat16 or wider, within the bound.
A program may use at most 128 MiB of HBM per device.

v0:
```python
import jax
import jax.numpy as jnp
from jax import lax
from jax.sharding import PartitionSpec as P

block_rows = 512


def sent_together(arrays, axis, dim, along):
    both = jnp.concatenate(arrays, axis=along)
    out, at, done = (lax.all_gather(both, axis, axis=dim, tiled=True), 0, [])
    for a in arrays:
        done.append(lax.slice_in_dim(out, at, at + a.shape[along], axis=along))
        at += a.shape[along]
    return tuple(done)


def attend(queries, keys, values, gates):
    length = queries.shape[0]
    scale = queries.shape[1] ** (-0.5)
    pieces = []
    for start in range(0, length, block_rows):
        finish = min(start + block_rows, length)
        scores = (
            jnp.dot(queries[start:finish], keys[:finish].T, preferred_element_type=jnp.float32)
            * scale
        )
        scores = scores + gates[start:finish, None] - gates[None, :finish]
        rows_at = start + lax.broadcasted_iota(jnp.int32, scores.shape, 0)
        cols_at = lax.broadcasted_iota(jnp.int32, scores.shape, 1)
        scores = jnp.where(cols_at <= rows_at, scores, -1e30)
        top = jnp.max(scores, axis=1, keepdims=True)
        weights = jnp.exp(scores - top)
        total = jnp.sum(weights, axis=1, keepdims=True)
        summed = jnp.dot(
            weights.astype(jnp.bfloat16), values[:finish], preferred_element_type=jnp.float32
        )
        pieces.append((summed / total).astype(jnp.bfloat16))
    return jnp.concatenate(pieces, axis=0)


def body(tokens, query_weight, key_weight, value_weight, cum_gate):
    width = query_weight.shape[1]
    full_query, full_key, full_value = sent_together(
        (query_weight, key_weight, value_weight), "dp", 0, 1
    )
    stacked = jnp.concatenate([full_query, full_key, full_value], axis=1)
    own_rows = tokens[0]
    projected = jnp.dot(
        lax.all_gather(own_rows, "sp", axis=0, tiled=True),
        stacked,
        preferred_element_type=jnp.float32,
    )
    queries = projected[:, :width].astype(jnp.bfloat16)
    keys = projected[:, width : 2 * width].astype(jnp.bfloat16)
    values = projected[:, 2 * width :].astype(jnp.bfloat16)
    head_out = attend(queries, keys, values, cum_gate[0, 0])
    gathered = lax.all_to_all(head_out, "sp", split_axis=0, concat_axis=1, tiled=True)
    return gathered[None]


def solution(mesh):
    in_specs = (
        P("dp", "sp", None),
        P("dp", "sp"),
        P("dp", "sp"),
        P("dp", "sp"),
        P("dp", "sp", None),
    )
    out_specs = P("dp", "sp", None)
    return jax.shard_map(body, mesh=mesh, in_specs=in_specs, out_specs=out_specs, check_vma=False)
```

profile of v0, /device:TPU:1, one launch (start us, length us, event | category | flops | bytes accessed | tf_op | source)
XLA Modules:
  0.0 272.2 jit_solution(10190009561996748113)
XLA Ops:
  6.5 1.6 pad_maximum_fusion
  8.1 0.0 all-gather.4.cloned.1.call-update
  8.2 0.0 all-gather.6.cloned.1.call-start
  8.2 0.7 all-gather.6.cloned.1.call-update
  9.0 0.7 slice_reduce_fusion.1
  9.7 0.7 slice_reduce_fusion
  10.4 0.8 fusion.100
  11.2 42.7 %all-gather.4.cloned.1.call-done = bf16[4096,384]{1,0:T(8,128)(2,1)} async-done(((bf16[256,384]{1,0:T(8,128)(2,1)}), bf16[4096,384]{1,0:T(8,128)(2,1)}) %all-gather.4.cloned.1.call-update) | async-done | bytes 3145744 | tf_op jit(solution)/shard_map/all_gather | solution.py:11
  53.9 159.6 %all-gather.6.cloned.1.call-done = bf16[1,3072,4096]{2,1,0:T(8,128)(2,1)} async-done(((bf16[1,192,4096]{2,1,0:T(8,128)(2,1)}), bf16[1,3072,4096]{2,1,0:T(8,128)(2,1)}) %all-gather.6.cloned.1.call-update) | async-done | bytes 25165840 | tf_op jit(solution)/shard_map/all_gather | solution.py:50
  213.5 16.0 %fusion.9 = bf16[3072,384]{0,1:T(8,128)(2,1)S(1)} fusion(bf16[4096,384]{1,0:T(8,128)(2,1)} %all-gather.4.cloned.1.call-done, bf16[1,3072,4096]{2,1,0:T(8,128)(2,1)} %all-gather.6.cloned.1.call-done), kind=kOutput, calls=%fused_computation.16 | convolution fusion | flops 9664856064 | bytes 30670848 | tf_op jit(solution)/shard_map/dot_general | solution.py:49
  229.5 0.0 slice-start
  229.6 0.4 fusion.101
  229.9 0.2 fusion.78
  230.1 0.4 fusion.43
  230.5 0.8 fusion.102
  231.3 0.5 fusion.28
  231.8 0.6 fusion.51
  232.4 1.1 fusion.103
  233.5 0.6 fusion.20
  234.0 0.7 fusion.47
  234.7 1.4 fusion.104
  236.1 0.7 fusion.12
  236.8 0.8 fusion.55
  237.7 1.6 fusion.105
  239.3 0.8 fusion.4
  240.1 1.0 fusion.64
  241.1 2.2 fusion.106
  243.3 1.0 fusion.2
  244.3 1.2 fusion.73
  245.4 18.2 %all_to_all.16 = bf16[16,192,128]{2,1,0:T(8,128)(2,1)S(1)} all-to-all(bf16[16,192,128]{2,1,0:T(8,128)(2,1)S(1)} %bitcast.22), channel_id=1, replica_groups=mesh['sp'=16,'dp'=16] {'sp'}, dimensions={0} | all-to-all | bytes 1572864 | tf_op jit(solution)/shard_map/all_to_all | solution.py:58
  263.7 0.5 copy.6
  264.2 1.2 broadcast_in_dim.31
  (11 shorter events, 0.0 us)
Async XLA Ops:
  6.5 47.4 %all-gather.4.cloned.1.call-start = ((), (), s32[]{:S(2)}) async-start(), calls=%async_computation.1 | async-start | bytes 3342336 | tf_op jit(solution)/shard_map/all_gather | solution.py:11
  8.2 205.4 %all-gather.6.cloned.1.call-start = ((), (), s32[]{:S(2)}) async-start(), calls=%async_computation.2 | async-start | bytes 26738688 | tf_op jit(solution)/shard_map/all_gather | solution.py:50
  229.5 1.0 slice-start
  233.4 1.3 slice-start.1
  240.1 1.0 copy-start
Sparse Core Ops, SparseCore 0:
  9.2 44.7 all-gather.3
  56.4 157.1 all-gather.5
where the time goes:
time: 273 us; the launch traced here: 272 us
  waiting for transfers between devices  203 us (74%)
  matrix products  28 us (10%)
  blocking collectives  18.2 us (7%)
  between operations  13.5 us (5%)
  other arithmetic  5.45 us (2%)
  local copies, waits for them, and re-layouts  3.96 us (1%)
    all_gather x1, waiting for transfers between devices, body(): lax.all_gather(own_rows, 'sp', axis=0, tiled=True)  160 us
    all_gather x1, waiting for transfers between devices, sent_together(): out, at, done = (lax.all_gather(both, axis, axis=dim, tiled=True), 0, [])  42.7 us
    all_to_all x1, blocking collectives, body(): lax.all_to_all(head_out, 'sp', split_axis=0, concat_axis=1, tiled=True)  18.2 us
    dot_general x1, matrix products, body(): jnp.dot(lax.all_gather(own_rows, 'sp', axis=0, tiled=True), stacked, pref...  16 us
    dot_general x6, matrix products, attend(): jnp.dot(queries[start:finish], keys[:finish].T, preferred_element_type=jn...  7.36 us
  transfers between devices with their start and end apart: 2, of which 2 were waited for; matrix products, arithmetic and copies ran while one was open for 1% of the time, Pallas kernels for 0%

commit v1 on v0

v1 whole, which is shorter than its diff:
```python
import functools
import heapq

import jax
import jax.numpy as jnp
from jax import lax
from jax.experimental import pallas as pl
from jax.experimental.pallas import tpu as pltpu
from jax.sharding import PartitionSpec as P

MESH = pl.DeviceIdType.MESH
NX, NY, NZ = 4, 4, 8
TOK, D, HEAD = 192, 4096, 128
QKV = 3 * HEAD
ROWS = 256
LEN = 3072
A_ROWS = 96
block_rows = 512

ORDER = (0, -1, 1, -2, 2, -3, 3, 4)


def weight_messages():
    a, b = A_ROWS * QKV * 2, (ROWS - A_ROWS) * QKV * 2
    m = {}
    for sign, link in ((1, "z+"), (-1, "z-")):
        for t in range(1, 5):
            half = 0.5 if t == 4 else 1.0
            m["Bz", sign, t] = (link, b * half, [("Bz", sign, t - 1)] if t > 1 else [])
    for k, off in enumerate(ORDER):
        if off == 0:
            need = []
        elif off == 4:
            need = [("Bz", 1, 4), ("Bz", -1, 4)]
        else:
            need = [("Bz", 1 if off < 0 else -1, abs(off))]
        m["By", 1, off] = ("y+", b, need)
        m["By", -1, off] = ("y-", b, need)
        m["Bf", 1, off] = ("y+", b / 2, [("By", 1, off)])
        m["Bf", -1, off] = ("y-", b / 2, [("By", -1, off)])
        m["Bd", 0, off] = ("d", b * 4, [("By", s, off) for s in (1, -1)] + [("Bf", s, off) for s in (1, -1)])
    m["Ay", 1, 0] = ("y+", a, [])
    m["Ay", -1, 0] = ("y-", a, [])
    m["Af", 1, 0] = ("y+", a / 2, [("Ay", 1, 0)])
    m["Af", -1, 0] = ("y-", a / 2, [("Ay", -1, 0)])
    first = [("Ay", 1, 0), ("Ay", -1, 0), ("Af", 1, 0), ("Af", -1, 0)]
    for sign, link in ((1, "z+"), (-1, "z-")):
        for t in range(1, 5):
            half = 0.5 if t == 4 else 1.0
            m["Az", sign, t] = (link, a * 4 * half, [("Az", sign, t - 1)] if t > 1 else first)
    for off in ORDER:
        if off == 0:
            need = first
        elif off == 4:
            need = [("Az", 1, 4), ("Az", -1, 4)]
        else:
            need = [("Az", 1 if off < 0 else -1, abs(off))]
        m["Ad", 0, off] = ("d", a * 4, need)
    return m


def token_messages():
    h = TOK * D
    return {
        ("T", 1, 0): ("x+", h, []),
        ("T", -1, 0): ("x-", h, []),
        ("T", 1, 1): ("x+", h, []),
        ("T", -1, 1): ("x-", h, []),
        ("T", 1, 2): ("x+", h, [("T", 1, 0)]),
        ("T", -1, 2): ("x-", h, [("T", -1, 0)]),
    }


def schedule(messages):
    rate = {"d": 600e3}
    free, arrive, order = {}, {}, []
    waiting = dict(messages)
    while waiting:
        ready = {}
        for name, (link, size, need) in waiting.items():
            if all(n in arrive for n in need):
                ready[name] = max([arrive[n] for n in need], default=0.0)
        name = min(ready, key=lambda n: (ready[n], list(messages).index(n)))
        link, size, need = waiting.pop(name)
        start = max(ready[name], free.get(link, 0.0))
        end = start + (size / rate["d"] if link == "d" else 2 * size / 90e3)
        free[link] = end
        arrive[name] = end + (1.0 if link == "d" else 1.8)
        order.append(name)
    return order, arrive


def report():
    m = {**weight_messages(), **token_messages()}
    order, arrive = schedule(m)
    for n in order:
        print(n, m[n][0], int(m[n][1]), round(arrive[n], 1))
    print(len(order))


def mo(v, n):
    return pl.multiple_of(v, n)


def kernel(tok, wq, wk, wv, out, w, t, p, q, relay, load_sem, send_sem, recv_sem):
    s, d = lax.axis_index("sp"), lax.axis_index("dp")
    y, x = lax.div(s, NX), lax.rem(s, NX)
    z, c = lax.div(d, 2), lax.rem(d, 2)

    def xs(i):
        return lax.rem(x + NX + i, NX)

    def ys(i):
        return lax.rem(y + NY + i, NY)

    def zs(i):
        return lax.rem(z + NZ + i, NZ)

    def dev(dx=0, dy=0, dz=0, other=False):
        return {"sp": ys(dy) * NX + xs(dx), "dp": zs(dz) * 2 + (1 - c if other else c)}

    loads = []
    for i, ref in enumerate((wq, wk, wv)):
        loads.append(pltpu.make_async_copy(
            ref, w.at[pl.ds(mo(d * ROWS, ROWS), ROWS), pl.ds(mo(y * QKV + i * HEAD, HEAD), HEAD)], load_sem.at[i]))
    loads.append(pltpu.make_async_copy(tok, t.at[x], load_sem.at[3]))
    for copy in loads:
        copy.start()

    barrier = pltpu.get_barrier_semaphore()
    greet = [dev(dx=1), dev(dx=-1), dev(dy=1), dev(dy=-1), dev(dz=1), dev(dz=-1), dev(other=True)]
    for who in greet:
        pl.semaphore_signal(barrier, inc=1, device_id=who, device_id_type=MESH)
    pl.semaphore_wait(barrier, len(greet))

    def wrect(zo, row0, rows, col=None, other=False):
        core = 1 - c if other else c
        at = pl.ds(mo((zs(zo) * 2 + core) * ROWS + row0, 16), rows)
        if col is None:
            return w.at[at]
        return w.at[at, pl.ds(mo(ys(col) * QKV, HEAD), QKV)]

    def regions(name):
        kind, sign, i = name
        row0, rows = (0, A_ROWS) if kind[0] == "A" else (A_ROWS, ROWS - A_ROWS)
        half = rows // 2
        if kind == "T":
            if i == 2:
                at = pl.ds(0 if sign == 1 else TOK // 2, TOK // 2)
                return t.at[xs(-sign), at], t.at[xs(-2 * sign), at], dev(dx=sign)
            at = pl.ds((0 if sign == 1 else TOK // 2) if i == 0 else (TOK // 2 if sign == 1 else 0), TOK // 2)
            return t.at[x, at], t.at[xs(-sign), at], dev(dx=sign)
        if kind in ("Az", "Bz"):
            col = None if kind == "Az" else 0
            if i == 4:
                row0, rows = row0 + (0 if sign == 1 else half), half
            return wrect(-sign * (i - 1), row0, rows, col), wrect(-sign * i, row0, rows, col), dev(dz=sign)
        if kind in ("Ay", "By"):
            return wrect(i, row0, rows, 0), wrect(i, row0, rows, -sign), dev(dy=sign)
        if kind in ("Af", "Bf"):
            row0, rows = row0 + (0 if sign == 1 else half), half
            return wrect(i, row0, rows, -sign), wrect(i, row0, rows, -2 * sign), dev(dy=sign)
        return wrect(i, row0, rows), wrect(i, row0, rows, other=True), dev(other=True)

    sent, arrived = [], set()
    number = {}

    def descriptor(src, dst, name, who):
        n = number.setdefault(name, len(number))
        return pltpu.make_async_remote_copy(
            src_ref=src, dst_ref=dst, send_sem=send_sem.at[n], recv_sem=recv_sem.at[n],
            device_id=who, device_id_type=MESH)

    def start(name, src, who, dst=None):
        copy = descriptor(src, src if dst is None else dst, name, who)
        copy.start()
        sent.append(copy)

    def arrival(name, where, who):
        if name not in arrived:
            arrived.add(name)
            descriptor(where, where, name, who).wait_recv()

    loaded = set()

    def load(*which):
        for i in which:
            if i not in loaded:
                loaded.add(i)
                loads[i].wait()

    messages = {**weight_messages(), **token_messages()}
    for name in schedule(messages)[0]:
        load(*((3,) if name[0] == "T" else (0, 1, 2)))
        for need in messages[name][2]:
            src, dst, who = regions(need)
            arrival(need, dst, who)
        src, dst, who = regions(name)
        start(name, src, who)
    for name in messages:
        if name[0] != "T":
            src, dst, who = regions(name)
            arrival(name, dst, who)

    def project(block):
        @pl.loop(0, NY * QKV // 256)
        def _(j):
            cols = pl.ds(mo(j * 256, 256), 256)
            p[block, :, cols] = jnp.dot(t[block], w[:, cols], preferred_element_type=jnp.float32).astype(jnp.bfloat16)

        q[y * NX + block] = p[block, :, pl.ds(mo(y * QKV, HEAD), QKV)]

    half = TOK // 2

    def exchange(n, block):
        for sign in (1, -1):
            rows = pl.ds(0 if sign == 1 else half, half)
            start(("Qr", sign, n), p.at[block, rows, pl.ds(mo(ys(2) * QKV, HEAD), QKV)], dev(dy=sign),
                  relay.at[block, 0 if sign == 1 else 1])
        for sign in (1, -1):
            start(("Qy", sign, n), p.at[block, :, pl.ds(mo(ys(sign) * QKV, HEAD), QKV)], dev(dy=sign),
                  q.at[y * NX + block])

    def forward(n, block):
        for sign in (1, -1):
            rows = pl.ds(0 if sign == 1 else half, half)
            place = relay.at[block, 0 if sign == 1 else 1]
            arrival(("Qr", sign, n), place, dev(dy=sign))
            start(("Qf", sign, n), place, dev(dy=sign), q.at[ys(-sign) * NX + block, rows])

    blocks = (xs(0), xs(-1), xs(1), xs(2))
    needs = ((), (("T", 1, 0), ("T", 1, 1)), (("T", -1, 0), ("T", -1, 1)), (("T", 1, 2), ("T", -1, 2)))
    for n, block in enumerate(blocks):
        for need in needs[n]:
            src, dst, who = regions(need)
            arrival(need, dst, who)
        project(block)
        exchange(n, block)
        if n > 0:
            forward(n - 1, blocks[n - 1])
    forward(3, blocks[3])
    for n, block in enumerate(blocks):
        for sign in (1, -1):
            rows = pl.ds(0 if sign == 1 else half, half)
            arrival(("Qy", sign, n), q.at[ys(-sign) * NX + block], dev(dy=sign))
            arrival(("Qf", sign, n), q.at[ys(-2 * sign) * NX + block, rows], dev(dy=sign))
    result = pltpu.make_async_copy(q, out, load_sem.at[4])
    result.start()
    for copy in sent:
        copy.wait_send()
    result.wait()


def attend(queries, keys, values, gates):
    length = queries.shape[0]
    scale = queries.shape[1] ** (-0.5)
    pieces = []
    for start in range(0, length, block_rows):
        finish = min(start + block_rows, length)
        scores = (
            jnp.dot(queries[start:finish], keys[:finish].T, preferred_element_type=jnp.float32)
            * scale
        )
        scores = scores + gates[start:finish, None] - gates[None, :finish]
        rows_at = start + lax.broadcasted_iota(jnp.int32, scores.shape, 0)
        cols_at = lax.broadcasted_iota(jnp.int32, scores.shape, 1)
        scores = jnp.where(cols_at <= rows_at, scores, -1e30)
        top = jnp.max(scores, axis=1, keepdims=True)
        weights = jnp.exp(scores - top)
        total = jnp.sum(weights, axis=1, keepdims=True)
        summed = jnp.dot(
            weights.astype(jnp.bfloat16), values[:finish], preferred_element_type=jnp.float32
        )
        pieces.append((summed / total).astype(jnp.bfloat16))
    return jnp.concatenate(pieces, axis=0)


def body(tokens, query_weight, key_weight, value_weight, cum_gate):
    count = len(weight_messages()) + len(token_messages()) + 24
    any_space = pl.BlockSpec(memory_space=pl.ANY)
    qkv = pl.pallas_call(
        kernel,
        out_shape=jax.ShapeDtypeStruct((NX * NY, TOK, QKV), jnp.bfloat16),
        in_specs=[any_space] * 4,
        out_specs=any_space,
        scratch_shapes=[
            pltpu.VMEM((D, NY * QKV), jnp.bfloat16),
            pltpu.VMEM((NX, TOK, D), jnp.bfloat16),
            pltpu.VMEM((NX, TOK, NY * QKV), jnp.bfloat16),
            pltpu.VMEM((NX * NY, TOK, QKV), jnp.bfloat16),
            pltpu.VMEM((NX, 2, TOK // 2, QKV), jnp.bfloat16),
            pltpu.SemaphoreType.DMA((5,)),
            pltpu.SemaphoreType.DMA((count,)),
            pltpu.SemaphoreType.DMA((count,)),
        ],
        compiler_params=pltpu.CompilerParams(
            collective_id=0, has_side_effects=True, vmem_limit_bytes=60 * 1024 * 1024
        ),
        name="gather_project",
    )(tokens[0], query_weight, key_weight, value_weight)
    qkv = qkv.reshape(LEN, QKV)
    head_out = attend(qkv[:, :HEAD], qkv[:, HEAD : 2 * HEAD], qkv[:, 2 * HEAD :], cum_gate[0, 0])
    gathered = lax.all_to_all(head_out, "sp", split_axis=0, concat_axis=1, tiled=True)
    return gathered[None]


def solution(mesh):
    in_specs = (
        P("dp", "sp", None),
        P("dp", "sp"),
        P("dp", "sp"),
        P("dp", "sp"),
        P("dp", "sp", None),
    )
    out_specs = P("dp", "sp", None)
    return jax.shard_map(body, mesh=mesh, in_specs=in_specs, out_specs=out_specs, check_vma=False)
```

time: 273 us -> 128 us (0.47)
  waiting for transfers between devices: 203 us -> 0 us
  Pallas kernels: 0 us -> 87.7 us
  matrix products: 28 us -> 13.6 us
  between operations: 13.5 us -> 0.11 us
    all_gather x2 -> x0, waiting for transfers between devices: 202 us -> none  [the longest x1 160 us: body(): lax.all_gather(own_rows, 'sp', axis=0, tiled=True)]
    pallas_call x0 -> x1, Pallas kernels: none -> 87.7 us  [body(): pl.pallas_call(kernel, out_shape=jax.ShapeDtypeStruct((NX * NY, TOK, QKV)...]
    dot_general x1 -> x0, matrix products: 16 us -> none  [body(): jnp.dot(lax.all_gather(own_rows, 'sp', axis=0, tiled=True), stacked, pref...]
  transfers between devices with their start and end apart: 2 -> 0, of which waited for: 2 -> 0; matrix products, arithmetic and copies ran while one was open for 1% -> 0% of each run, Pallas kernels for 0% -> 0%
where the time goes in v1:
time: 128 us
  Pallas kernels  87.7 us (69%)
  blocking collectives  18.6 us (15%)
  matrix products  13.6 us (11%)
  local copies, waits for them, and re-layouts  3.96 us (3%)
  other arithmetic  3.85 us (3%)
    pallas_call x1, Pallas kernels, body(): pl.pallas_call(kernel, out_shape=jax.ShapeDtypeStruct((NX * NY, TOK, QKV)...  87.7 us
    all_to_all x1, blocking collectives, body(): lax.all_to_all(head_out, 'sp', split_axis=0, concat_axis=1, tiled=True)  18.6 us
    dot_general x6, matrix products, attend(): jnp.dot(queries[start:finish], keys[:finish].T, preferred_element_type=jn...  8.13 us
    dot_general x6, matrix products, attend(): jnp.dot(weights.astype(jnp.bfloat16), values[:finish], preferred_element_...  5.46 us
    reduce_sum x6, other arithmetic, attend(): total = jnp.sum(weights, axis=1, keepdims=True)  3.83 us

profile of v1, /device:TPU:1, one launch (start us, length us, event | category | flops | bytes accessed | tf_op | source)
XLA Modules:
  0.0 127.8 jit_solution(8133401271823647582)
XLA Ops:
  0.0 0.7 slice_reduce_fusion.1
  0.8 0.7 slice_reduce_fusion
  1.5 0.8 fusion.92
  2.3 87.7 %gather_project.1 = bf16[16,192,384]{2,1,0:T(8,128)(2,1)} custom-call(bf16[192,4096]{1,0:T(8,128)(2,1)} %bitcast.26, bf16[256,128]{1,0:T(8,128)(2,1)} %wq.1, bf16[256,128]{1,0:T(8,128)(2,1)} %wk.1, bf16[256,128]{1,0:T(8,128)(2,1)} %wv.1), custom_call_target="tpu_custom_call" | custom-call | tf_op jit(solution)/shard_map/gather_project/pallas_call | solution.py:281
  90.0 0.0 copy-start
  90.0 0.0 slice-start
  90.0 1.4 %fusion.93 = (f32[512]{0:T(512)S(1)}, f32[512,512]{0,1:T(8,128)S(1)}) fusion(f32[512]{0:T(512)S(1)} %bitcast.36, bf16[3072,384]{1,0:T(8,128)(2,1)} %bitcast.13), kind=kOutput, calls=%fused_computation.90 | convolution fusion | flops 68681216 | bytes 1316864 | tf_op jit(solution)/shard_map/dot_general | solution.py:261
  91.4 0.2 fusion.70
  91.6 1.3 fusion.35
  92.9 0.0 copy-done
  92.9 0.0 slice-done
  92.9 0.7 fusion.94
  93.6 0.5 fusion.20
  94.2 0.6 fusion.43
  94.7 1.0 fusion.95
  95.7 0.0 slice-start.1
  95.7 0.6 fusion.12
  96.3 0.7 fusion.39
  97.0 0.0 slice-done.1
  97.0 1.3 %fusion.96 = (f32[512]{0:T(512)S(1)}, f32[512,2048]{1,0:T(8,128)S(1)}) fusion(f32[2048]{0:T(1024)S(1)} %bitcast.30, f32[512]{0:T(512)S(1)} %bitcast.33, bf16[3072,384]{1,0:T(8,128)(2,1)S(1)} %bitcast.19, s32[512]{0:T(512)S(1)} %iota_add_fusion.2), kind=kOutput, calls=%fused_computation.93 | convolution fusion | flops 274726400 | bytes 4864000 | tf_op jit(solution)/shard_map/dot_general | solution.py:261
  98.3 0.7 fusion.4
  99.0 0.9 fusion.47
  99.9 1.6 %fusion.97 = (f32[512]{0:T(512)S(1)}, f32[512,2560]{1,0:T(8,128)S(1)}) fusion(f32[2560]{0:T(1024)S(1)} %slice_reduce_fusion, f32[512]{0:T(512)S(1)} %bitcast.32, bf16[3072,384]{1,0:T(8,128)(2,1)S(1)} %bitcast.21, s32[512]{0:T(512)S(1)} %iota_add_fusion.1), kind=kOutput, calls=%fused_computation.94 | convolution fusion | flops 343408128 | bytes 6047744 | tf_op jit(solution)/shard_map/dot_general | solution.py:261
  101.4 0.8 fusion.2
  102.3 1.0 fusion.56
  103.3 0.0 copy-done.1
  103.3 2.1 %fusion.98 = (f32[512]{0:T(512)S(1)}, f32[512,3072]{1,0:T(8,128)S(1)}) fusion(f32[3072]{0:T(1024)S(1)} %bitcast.28, f32[512]{0:T(512)S(1)} %bitcast.31, bf16[3072,384]{1,0:T(8,128)(2,1)S(1)} %bitcast.23, s32[512]{0:T(512)S(1)} %iota_add_fusion), kind=kOutput, calls=%fused_computation.95 | convolution fusion | flops 412089856 | bytes 7227392 | tf_op jit(solution)/shard_map/dot_general | solution.py:261
  105.4 1.0 fusion
  106.4 1.1 fusion.65
  107.5 18.6 %all_to_all.16 = bf16[16,192,128]{2,1,0:T(8,128)(2,1)S(1)} all-to-all(bf16[16,192,128]{2,1,0:T(8,128)(2,1)S(1)} %bitcast.27), channel_id=1, replica_groups=mesh['sp'=16,'dp'=16] {'sp'}, dimensions={0} | all-to-all | bytes 1572864 | tf_op jit(solution)/shard_map/all_to_all | solution.py:303
  126.1 0.5 copy.6
  126.6 1.2 broadcast_in_dim.31
  (6 shorter events, 0.0 us)
Async XLA Ops:
  90.0 2.9 %copy-start = (bf16[16,192,384]{2,1,0:T(8,128)(2,1)S(1)}, bf16[16,192,384]{2,1,0:T(8,128)(2,1)}, u32[]{:S(2)}) copy-start(bf16[16,192,384]{2,1,0:T(8,128)(2,1)} %gather_project.1) | copy-start | bytes 7077892
  90.0 2.9 %slice-start = ((f32[1,1,3072]{2,1,0:T(1,128)}), f32[1,1,1024]{2,1,0:T(1,128)S(1)}, s32[]{:S(2)}) async-start(f32[1,1,3072]{2,1,0:T(1,128)} %param.9), calls=%async_computation.1 | async-start | bytes 8192 | tf_op jit(solution)/shard_map/slice | solution.py:264
  95.7 1.3 %slice-start.1 = ((f32[1,1,3072]{2,1,0:T(1,128)}), f32[1,1,2048]{2,1,0:T(1,128)S(1)}, s32[]{:S(2)}) async-start(f32[1,1,3072]{2,1,0:T(1,128)} %param.9), calls=%async_computation.2 | async-start | bytes 16384 | tf_op jit(solution)/shard_map/slice | solution.py:264
  102.3 1.0 copy-start.1

commit v2 on v1

--- a/solution.py
+++ b/solution.py
@@ -15,7 +15,8 @@
 ROWS = 256
 LEN = 3072
 A_ROWS = 96
-block_rows = 512
+Q_ROWS, K_ROWS = 384, 768
+LOG2E = 1.4426950408889634
 
 ORDER = (0, -1, 1, -2, 2, -3, 3, 4)
 
@@ -102,7 +103,7 @@
     return pl.multiple_of(v, n)
 
 
-def kernel(tok, wq, wk, wv, out, w, t, p, q, relay, load_sem, send_sem, recv_sem):
+def kernel(tok, wq, wk, wv, gate, out, w, t, p, q, relay, bias, scores, head_out, load_sem, send_sem, recv_sem, out_send, out_recv):
     s, d = lax.axis_index("sp"), lax.axis_index("dp")
     y, x = lax.div(s, NX), lax.rem(s, NX)
     z, c = lax.div(d, 2), lax.rem(d, 2)
@@ -128,7 +129,8 @@
         copy.start()
 
     barrier = pltpu.get_barrier_semaphore()
-    greet = [dev(dx=1), dev(dx=-1), dev(dy=1), dev(dy=-1), dev(dz=1), dev(dz=-1), dev(other=True)]
+    greet = [dev(dx=dx, dy=dy) for dy in range(NY) for dx in range(NX) if dx or dy]
+    greet += [dev(dz=1), dev(dz=-1), dev(other=True)]
     for who in greet:
         pl.semaphore_signal(barrier, inc=1, device_id=who, device_id_type=MESH)
     pl.semaphore_wait(barrier, len(greet))
@@ -202,13 +204,16 @@
             src, dst, who = regions(name)
             arrival(name, dst, who)
 
+    def tokens_of(row, block, at=0, count=TOK):
+        return pl.ds(mo((row * NX + block) * TOK + at, 16), count)
+
     def project(block):
         @pl.loop(0, NY * QKV // 256)
         def _(j):
             cols = pl.ds(mo(j * 256, 256), 256)
             p[block, :, cols] = jnp.dot(t[block], w[:, cols], preferred_element_type=jnp.float32).astype(jnp.bfloat16)
 
-        q[y * NX + block] = p[block, :, pl.ds(mo(y * QKV, HEAD), QKV)]
+        q[tokens_of(y, block)] = p[block, :, pl.ds(mo(y * QKV, HEAD), QKV)]
 
     half = TOK // 2
 
@@ -219,14 +224,13 @@
                   relay.at[block, 0 if sign == 1 else 1])
         for sign in (1, -1):
             start(("Qy", sign, n), p.at[block, :, pl.ds(mo(ys(sign) * QKV, HEAD), QKV)], dev(dy=sign),
-                  q.at[y * NX + block])
+                  q.at[tokens_of(y, block)])
 
     def forward(n, block):
         for sign in (1, -1):
-            rows = pl.ds(0 if sign == 1 else half, half)
             place = relay.at[block, 0 if sign == 1 else 1]
             arrival(("Qr", sign, n), place, dev(dy=sign))
-            start(("Qf", sign, n), place, dev(dy=sign), q.at[ys(-sign) * NX + block, rows])
+            start(("Qf", sign, n), place, dev(dy=sign), q.at[tokens_of(ys(-sign), block, 0 if sign == 1 else half, half)])
 
     blocks = (xs(0), xs(-1), xs(1), xs(2))
     needs = ((), (("T", 1, 0), ("T", 1, 1)), (("T", -1, 0), ("T", -1, 1)), (("T", 1, 2), ("T", -1, 2)))
@@ -241,67 +245,116 @@
     forward(3, blocks[3])
     for n, block in enumerate(blocks):
         for sign in (1, -1):
-            rows = pl.ds(0 if sign == 1 else half, half)
-            arrival(("Qy", sign, n), q.at[ys(-sign) * NX + block], dev(dy=sign))
-            arrival(("Qf", sign, n), q.at[ys(-2 * sign) * NX + block, rows], dev(dy=sign))
-    result = pltpu.make_async_copy(q, out, load_sem.at[4])
-    result.start()
+            arrival(("Qy", sign, n), q.at[tokens_of(ys(-sign), block)], dev(dy=sign))
+            arrival(("Qf", sign, n), q.at[tokens_of(ys(-2 * sign), block, 0 if sign == 1 else half, half)], dev(dy=sign))
+
+    bias[...] = gate[...] * LOG2E
+
+    def give(block):
+        rows = head_out.at[pl.ds(block * TOK, TOK)]
+        place = out.at[:, pl.ds(mo(s * HEAD, HEAD), HEAD)]
+
+        @pl.when(s != block)
+        def _():
+            pltpu.make_async_remote_copy(
+                src_ref=rows, dst_ref=place, send_sem=out_send.at[block], recv_sem=out_recv.at[s],
+                device_id={"sp": block, "dp": d}, device_id_type=MESH).start()
+
+        @pl.when(s == block)
+        def _():
+            pltpu.make_async_copy(rows, place, load_sem.at[4]).start()
+
+    @pl.loop(0, LEN // Q_ROWS)
+    def _(step):
+        now = lax.rem(lax.div(s, 2) + step, LEN // Q_ROWS)
+        for i in range(LEN // Q_ROWS):
+            @pl.when(now == i)
+            def _():
+                attend_rows(i, q, bias, scores, head_out)
+                for block in range(i * Q_ROWS // TOK, (i + 1) * Q_ROWS // TOK):
+                    give(block)
+
     for copy in sent:
         copy.wait_send()
-    result.wait()
-
-
-def attend(queries, keys, values, gates):
-    length = queries.shape[0]
-    scale = queries.shape[1] ** (-0.5)
-    pieces = []
-    for start in range(0, length, block_rows):
-        finish = min(start + block_rows, length)
-        scores = (
-            jnp.dot(queries[start:finish], keys[:finish].T, preferred_element_type=jnp.float32)
-            * scale
-        )
-        scores = scores + gates[start:finish, None] - gates[None, :finish]
-        rows_at = start + lax.broadcasted_iota(jnp.int32, scores.shape, 0)
-        cols_at = lax.broadcasted_iota(jnp.int32, scores.shape, 1)
-        scores = jnp.where(cols_at <= rows_at, scores, -1e30)
-        top = jnp.max(scores, axis=1, keepdims=True)
-        weights = jnp.exp(scores - top)
-        total = jnp.sum(weights, axis=1, keepdims=True)
-        summed = jnp.dot(
-            weights.astype(jnp.bfloat16), values[:finish], preferred_element_type=jnp.float32
-        )
-        pieces.append((summed / total).astype(jnp.bfloat16))
-    return jnp.concatenate(pieces, axis=0)
+    for block in range(NX * NY):
+        rows = head_out.at[pl.ds(block * TOK, TOK)]
+
+        @pl.when(s != block)
+        def _():
+            copy = pltpu.make_async_remote_copy(
+                src_ref=rows, dst_ref=out.at[:, pl.ds(block * HEAD, HEAD)], send_sem=out_send.at[block],
+                recv_sem=out_recv.at[block], device_id={"sp": block, "dp": d}, device_id_type=MESH)
+            copy.wait_send()
+            copy.wait_recv()
+
+        @pl.when(s == block)
+        def _():
+            pltpu.make_async_copy(rows, out.at[:, pl.ds(block * HEAD, HEAD)], load_sem.at[4]).wait()
+
+
+def fold(a, op):
+    return functools.reduce(op, [a[:, i : i + 128] for i in range(0, a.shape[1], 128)])
+
+
+def attend_rows(i, q, bias, scores, head_out):
+    first, last = i * Q_ROWS, (i + 1) * Q_ROWS
+    queries = q[first:last, :HEAD]
+    base = bias[0:1, first : first + 1]
+    scale = HEAD**-0.5 * LOG2E
+    cuts = [(at, min(at + K_ROWS, last)) for at in range(0, last, K_ROWS)]
+    top = None
+    for at, end in cuts:
+        part = lax.dot_general(queries, q[at:end, HEAD : 2 * HEAD], (((1,), (1,)), ((), ())),
+                               preferred_element_type=jnp.float32)
+        part = part * scale + (base - bias[0:1, at:end])
+        if end > first:
+            rows_at = first + lax.broadcasted_iota(jnp.int32, part.shape, 0)
+            cols_at = at + lax.broadcasted_iota(jnp.int32, part.shape, 1)
+            part = jnp.where(cols_at <= rows_at, part, -1e30)
+        scores[:, at:end] = part
+        high = fold(part, jnp.maximum)
+        top = high if top is None else jnp.maximum(top, high)
+    top = jnp.max(top, axis=1, keepdims=True)
+    total = summed = None
+    for at, end in cuts:
+        weights = jnp.exp2(scores[:, at:end] - top)
+        low = fold(weights, jnp.add)
+        part = jnp.dot(weights.astype(jnp.bfloat16), q[at:end, 2 * HEAD :], preferred_element_type=jnp.float32)
+        total = low if total is None else total + low
+        summed = part if summed is None else summed + part
+    head_out[first:last] = (summed / jnp.sum(total, axis=1, keepdims=True)).astype(jnp.bfloat16)
 
 
 def body(tokens, query_weight, key_weight, value_weight, cum_gate):
     count = len(weight_messages()) + len(token_messages()) + 24
     any_space = pl.BlockSpec(memory_space=pl.ANY)
-    qkv = pl.pallas_call(
+    vmem_space = pl.BlockSpec(memory_space=pltpu.VMEM)
+    attended = pl.pallas_call(
         kernel,
-        out_shape=jax.ShapeDtypeStruct((NX * NY, TOK, QKV), jnp.bfloat16),
-        in_specs=[any_space] * 4,
+        out_shape=jax.ShapeDtypeStruct((TOK, NX * NY * HEAD), jnp.bfloat16),
+        in_specs=[any_space] * 4 + [vmem_space],
         out_specs=any_space,
         scratch_shapes=[
             pltpu.VMEM((D, NY * QKV), jnp.bfloat16),
             pltpu.VMEM((NX, TOK, D), jnp.bfloat16),
             pltpu.VMEM((NX, TOK, NY * QKV), jnp.bfloat16),
-            pltpu.VMEM((NX * NY, TOK, QKV), jnp.bfloat16),
+            pltpu.VMEM((LEN, QKV), jnp.bfloat16),
             pltpu.VMEM((NX, 2, TOK // 2, QKV), jnp.bfloat16),
+            pltpu.VMEM((1, LEN), jnp.float32),
+            pltpu.VMEM((Q_ROWS, LEN), jnp.float32),
+            pltpu.VMEM((LEN, HEAD), jnp.bfloat16),
             pltpu.SemaphoreType.DMA((5,)),
             pltpu.SemaphoreType.DMA((count,)),
             pltpu.SemaphoreType.DMA((count,)),
+            pltpu.SemaphoreType.DMA((NX * NY,)),
+            pltpu.SemaphoreType.DMA((NX * NY,)),
         ],
         compiler_params=pltpu.CompilerParams(
             collective_id=0, has_side_effects=True, vmem_limit_bytes=60 * 1024 * 1024
         ),
-        name="gather_project",
-    )(tokens[0], query_weight, key_weight, value_weight)
-    qkv = qkv.reshape(LEN, QKV)
-    head_out = attend(qkv[:, :HEAD], qkv[:, HEAD : 2 * HEAD], qkv[:, 2 * HEAD :], cum_gate[0, 0])
-    gathered = lax.all_to_all(head_out, "sp", split_axis=0, concat_axis=1, tiled=True)
-    return gathered[None]
+        name="mixer",
+    )(tokens[0], query_weight, key_weight, value_weight, cum_gate[0])
+    return attended[None]
 
 
 def solution(mesh):

time: 128 us -> 113 us (0.88)
  Pallas kernels: 87.7 us -> 111 us
  blocking collectives: 18.6 us -> 0 us
  matrix products: 13.6 us -> 0 us
  other arithmetic: 3.85 us -> 0 us
  local copies, waits for them, and re-layouts: 3.96 us -> 2.09 us
    pallas_call x1, Pallas kernels: 87.7 us -> 111 us  [body(): pl.pallas_call(kernel, out_shape=jax.ShapeDtypeStruct((TOK, NX * NY * HEA...]
    all_to_all x1 -> x0, blocking collectives: 18.6 us -> none  [body(): lax.all_to_all(head_out, 'sp', split_axis=0, concat_axis=1, tiled=True)]
    dot_general x12 -> x0, matrix products: 13.6 us -> none  [the longest x6 8.13 us: attend(): jnp.dot(queries[start:finish], keys[:finish].T, preferred_element_type=jn...]
    reduce_sum x6 -> x0, other arithmetic: 3.83 us -> none  [attend(): total = jnp.sum(weights, axis=1, keepdims=True)]
    slice x7 -> x0, local copies, waits for them, and re-layouts: 2.23 us -> none  [attend(): scores = scores + gates[start:finish, None] - gates[None, :finish]]
    unnamed x4 -> x1, local copies, waits for them, and re-layouts: 0.01 us -> 2.09 us
where the time goes in v2:
time: 113 us
  Pallas kernels  111 us (98%)
  local copies, waits for them, and re-layouts  2.09 us (2%)
    pallas_call x1, Pallas kernels, body(): pl.pallas_call(kernel, out_shape=jax.ShapeDtypeStruct((TOK, NX * NY * HEA...  111 us

profile of v2, /device:TPU:1, one launch (start us, length us, event | category | flops | bytes accessed | tf_op | source)
XLA Modules:
  0.0 112.9 jit_solution(4216332763659406960)
XLA Ops:
  0.0 110.8 %mixer.1 = bf16[192,2048]{1,0:T(8,128)(2,1)} custom-call(bf16[192,4096]{1,0:T(8,128)(2,1)} %bitcast.4, bf16[256,128]{1,0:T(8,128)(2,1)} %wq.1, bf16[256,128]{1,0:T(8,128)(2,1)} %wk.1, bf16[256,128]{1,0:T(8,128)(2,1)} %wv.1, f32[1,3072]{1,0:T(1,128)} %bitcast.5), custom_call_target="tpu_custom_call" | custom-call | tf_op jit(solution)/shard_map/mixer/pallas_call | solution.py:332
  110.8 2.1 %copy.7 = bf16[1,192,2048]{2,1,0:T(8,128)(2,1)} copy(bf16[1,192,2048]{2,1,0:T(8,128)(2,1)} %bitcast.3) | data formatting | bytes 1572864

commit v3 on v2

--- a/solution.py
+++ b/solution.py
@@ -24,6 +24,10 @@
 def weight_messages():
     a, b = A_ROWS * QKV * 2, (ROWS - A_ROWS) * QKV * 2
     m = {}
+    m["Ay", 1, 0] = ("y+", a, [])
+    m["Ay", -1, 0] = ("y-", a, [])
+    m["Af", 1, 0] = ("y+", a / 2, [("Ay", 1, 0)])
+    m["Af", -1, 0] = ("y-", a / 2, [("Ay", -1, 0)])
     for sign, link in ((1, "z+"), (-1, "z-")):
         for t in range(1, 5):
             half = 0.5 if t == 4 else 1.0
@@ -40,10 +44,6 @@
         m["Bf", 1, off] = ("y+", b / 2, [("By", 1, off)])
         m["Bf", -1, off] = ("y-", b / 2, [("By", -1, off)])
         m["Bd", 0, off] = ("d", b * 4, [("By", s, off) for s in (1, -1)] + [("Bf", s, off) for s in (1, -1)])
-    m["Ay", 1, 0] = ("y+", a, [])
-    m["Ay", -1, 0] = ("y-", a, [])
-    m["Af", 1, 0] = ("y+", a / 2, [("Ay", 1, 0)])
-    m["Af", -1, 0] = ("y-", a / 2, [("Ay", -1, 0)])
     first = [("Ay", 1, 0), ("Ay", -1, 0), ("Af", 1, 0), ("Af", -1, 0)]
     for sign, link in ((1, "z+"), (-1, "z-")):
         for t in range(1, 5):
@@ -252,7 +252,7 @@
 
     def give(block):
         rows = head_out.at[pl.ds(block * TOK, TOK)]
-        place = out.at[:, pl.ds(mo(s * HEAD, HEAD), HEAD)]
+        place = out.at[s]
 
         @pl.when(s != block)
         def _():
@@ -282,14 +282,14 @@
         @pl.when(s != block)
         def _():
             copy = pltpu.make_async_remote_copy(
-                src_ref=rows, dst_ref=out.at[:, pl.ds(block * HEAD, HEAD)], send_sem=out_send.at[block],
+                src_ref=rows, dst_ref=out.at[block], send_sem=out_send.at[block],
                 recv_sem=out_recv.at[block], device_id={"sp": block, "dp": d}, device_id_type=MESH)
             copy.wait_send()
             copy.wait_recv()
 
         @pl.when(s == block)
         def _():
-            pltpu.make_async_copy(rows, out.at[:, pl.ds(block * HEAD, HEAD)], load_sem.at[4]).wait()
+            pltpu.make_async_copy(rows, out.at[block], load_sem.at[4]).wait()
 
 
 def fold(a, op):
@@ -325,13 +325,25 @@
     head_out[first:last] = (summed / jnp.sum(total, axis=1, keepdims=True)).astype(jnp.bfloat16)
 
 
+def merge(heads, out, held, sem):
+    come = [pltpu.make_async_copy(heads.at[i], held.at[i], sem.at[0, i]) for i in range(NX * NY)]
+    go = [pltpu.make_async_copy(held.at[i], out.at[:, pl.ds(i * HEAD, HEAD)], sem.at[1, i]) for i in range(NX * NY)]
+    for copy in come:
+        copy.start()
+    for one, other in zip(come, go):
+        one.wait()
+        other.start()
+    for copy in go:
+        copy.wait()
+
+
 def body(tokens, query_weight, key_weight, value_weight, cum_gate):
     count = len(weight_messages()) + len(token_messages()) + 24
     any_space = pl.BlockSpec(memory_space=pl.ANY)
     vmem_space = pl.BlockSpec(memory_space=pltpu.VMEM)
     attended = pl.pallas_call(
         kernel,
-        out_shape=jax.ShapeDtypeStruct((TOK, NX * NY * HEAD), jnp.bfloat16),
+        out_shape=jax.ShapeDtypeStruct((NX * NY, TOK, HEAD), jnp.bfloat16),
         in_specs=[any_space] * 4 + [vmem_space],
         out_specs=any_space,
         scratch_shapes=[
@@ -354,7 +366,15 @@
         ),
         name="mixer",
     )(tokens[0], query_weight, key_weight, value_weight, cum_gate[0])
-    return attended[None]
+    merged = pl.pallas_call(
+        merge,
+        out_shape=jax.ShapeDtypeStruct((TOK, NX * NY * HEAD), jnp.bfloat16),
+        in_specs=[any_space],
+        out_specs=any_space,
+        scratch_shapes=[pltpu.VMEM((NX * NY, TOK, HEAD), jnp.bfloat16), pltpu.SemaphoreType.DMA((2, NX * NY))],
+        name="merge",
+    )(attended)
+    return merged[None]
 
 
 def solution(mesh):

time: 113 us -> 104 us (0.920)
  Pallas kernels: 111 us -> 103 us
  local copies, waits for them, and re-layouts: 2.09 us -> 0 us
    pallas_call x1 -> x2, Pallas kernels: 111 us -> 103 us  [the longest x1 101 us: body(): pl.pallas_call(kernel, out_shape=jax.ShapeDtypeStruct((NX * NY, TOK, HEAD...]
    unnamed x1 -> x0, local copies, waits for them, and re-layouts: 2.09 us -> none
where the time goes in v3:
time: 104 us
  Pallas kernels  103 us (99%)
    pallas_call x1, Pallas kernels, body(): pl.pallas_call(kernel, out_shape=jax.ShapeDtypeStruct((NX * NY, TOK, HEAD...  101 us

profile of v3, /device:TPU:1, one launch (start us, length us, event | category | flops | bytes accessed | tf_op | source)
XLA Modules:
  0.0 103.6 jit_solution(1405876624110411802)
XLA Ops:
  0.0 101.4 %mixer.1.heads = bf16[16,192,128]{2,1,0:T(8,128)(2,1)} custom-call(bf16[192,4096]{1,0:T(8,128)(2,1)} %bitcast.3, bf16[256,128]{1,0:T(8,128)(2,1)} %wq.1, bf16[256,128]{1,0:T(8,128)(2,1)} %wk.1, bf16[256,128]{1,0:T(8,128)(2,1)} %wv.1, f32[1,3072]{1,0:T(1,128)} %bitcast.4), custom_call_target="tpu_custom_call" | custom-call | tf_op jit(solution)/shard_map/mixer/pallas_call | solution.py:344
  101.4 2.0 %merge.1 = bf16[192,2048]{1,0:T(8,128)(2,1)} custom-call(bf16[16,192,128]{2,1,0:T(8,128)(2,1)} %mixer.1.heads), custom_call_target="tpu_custom_call" | custom-call | tf_op jit(solution)/shard_map/merge/pallas_call | solution.py:369

commit v4 on v0

v4 whole, which is shorter than its diff:
```python
import functools

import jax
import jax.numpy as jnp
from jax import lax
from jax.experimental import pallas as pl
from jax.experimental.pallas import tpu as pltpu
from jax.sharding import PartitionSpec as P

MESH = pl.DeviceIdType.MESH
NX, NY, NZ = 4, 4, 8
TOK, D, HEAD = 192, 4096, 128
HALF = TOK // 2
ROWS = 256
LEN = 3072
GROUP = NY * TOK
LOG2E = 1.4426950408889634

QKV = 3 * HEAD
A_ROWS = 96
ORDER = (0, -1, 1, -2, 2, -3, 3, 4)
OFF = (0, -1, 1, 2)
BATCHES = ((0, 1, 2), (3,))
TILE_US, PAIR_US = (1.4, 0.65), 0.9
TILES = (3, 4, 5, 2, 1, 0)


def weight_messages():
    a, b, g = A_ROWS * QKV * 2, (ROWS - A_ROWS) * QKV * 2, 0
    m = {}
    for sign, link in ((1, "y+"), (-1, "y-")):
        m["Ay", g, sign, 0] = (link, a, [])
    for sign, link in ((1, "y+"), (-1, "y-")):
        m["Af", g, sign, 0] = (link, a / 2, [("Ay", g, sign, 0)])
    first = [(kind, g, sign, 0) for kind in ("Ay", "Af") for sign in (1, -1)]

    def along_z(kind, size, need):
        for sign, link in ((1, "z+"), (-1, "z-")):
            for t in range(1, 5):
                m[kind, g, sign, t] = (link, size * (0.5 if t == 4 else 1), [(kind, g, sign, t - 1)] if t > 1 else need)

    def block(kind, off, own):
        if off == 0:
            return own
        if off == 4:
            return [(kind, g, 1, 4), (kind, g, -1, 4)]
        return [(kind, g, 1 if off < 0 else -1, abs(off))]

    if b:
        along_z("Bz", b, [])
        for off in ORDER:
            need = block("Bz", off, [])
            for sign, link in ((1, "y+"), (-1, "y-")):
                m["By", g, sign, off] = (link, b, need)
                m["Bf", g, sign, off] = (link, b / 2, [("By", g, sign, off)])
            m["Bd", g, 0, off] = ("d", b * 4, [(kind, g, sign, off) for kind in ("By", "Bf") for sign in (1, -1)])
    along_z("Az", a * 4, first)
    for off in ORDER:
        m["Ad", g, 0, off] = ("d", a * 4, block("Az", off, first))
    return m


def token_messages():
    h = HALF * D * 2
    m = {}
    for i in range(3):
        for sign, link in ((1, "x+"), (-1, "x-")):
            m["T", 0, sign, i] = (link, h, [("T", 0, sign, 0)] if i == 2 else [])
    return m


def batch_of(n):
    return next(i for i, batch in enumerate(BATCHES) if n in batch)


def exchange_messages(n):
    m = {}
    size = TOK * QKV * 2
    for sign, link in ((1, "y+"), (-1, "y-")):
        m["Er", 0, sign, n] = (link, size / 2, [("tile", batch_of(n), 3), ("tile", batch_of(n), 4)])
        m["Ef", 0, sign, n] = (link, size / 2, [("Er", 0, sign, n)])
        m["Ey", 0, sign, n] = (link, size, [("tile", batch_of(n), 5 if sign < 0 else 1)])
    return m


def tasks():
    t = {}
    tokens = ([], [("T", 0, 1, 0), ("T", 0, 1, 1)], [("T", 0, -1, 0), ("T", 0, -1, 1)], [("T", 0, 1, 2), ("T", 0, -1, 2)])
    for i, batch in enumerate(BATCHES):
        for j in TILES:
            need = [k for n in batch for k in tokens[n]] + list(weight_messages())
            t["tile", i, j] = (TILE_US[i], need)
    done = [[(kind, 0, sign, n) for kind in ("Ey", "Ef") for sign in (1, -1)] for n in range(NX)]
    last = NX - 1
    order = [(m, n) for m in range(last) for n in range(last)]
    order += [(last, n) for n in range(NX)] + [(m, last) for m in (1, 2, 0)]
    for m, n in order:
        t["pair", m, n] = (PAIR_US, done[n] + done[m])
    names = list(t)
    for before, name in zip(names, names[1:]):
        t[name][1].append(before)
    return t


def schedule():
    messages = {}
    for some in (weight_messages(), token_messages(), *(exchange_messages(n) for n in range(NX))):
        messages.update(some)
    work = tasks()
    place = {name: i for i, name in enumerate([*messages, *work])}
    done, free, order, now = {}, {}, [], 0.0
    left = dict.fromkeys(place)
    while left:
        ready = []
        for name in left:
            need = messages[name][2] if name in messages else work[name][1]
            if all(k in done for k in need):
                at = max([done[k] for k in need], default=0.0)
                ready.append((max(at, now), name in work, at if name in messages else 0.0, place[name], name))
        at, heavy, _, _, name = min(ready)
        del left[name]
        order.append(name)
        now = at
        if heavy:
            now += work[name][0]
            done[name] = now
        else:
            link, size, _ = messages[name]
            end = max(now, free.get(link, 0.0)) + (size / 600e3 if link == "d" else size / 45e3)
            free[link] = end
            done[name] = end + (1.0 if link == "d" else 1.8)
    return order, messages, work, done, free


def mo(v, n):
    return pl.multiple_of(v, n)


def fold(parts, op):
    return functools.reduce(op, parts)


def kernel(tok, wq, wk, wv, gate, out, w, t, p, relay, qkv, bias, high, total, summed, heads,
           load_sem, send_sem, recv_sem):
    s, d = lax.axis_index("sp"), lax.axis_index("dp")
    y, x = lax.div(s, NX), lax.rem(s, NX)
    z, c = lax.div(d, 2), lax.rem(d, 2)

    def xs(i):
        return lax.rem(x + NX + i, NX)

    def ys(i):
        return lax.rem(y + NY + i, NY)

    def zs(i):
        return lax.rem(z + NZ + i, NZ)

    def dev(dx=0, dy=0, dz=0, other=False):
        return {"sp": ys(dy) * NX + xs(dx), "dp": zs(dz) * 2 + (1 - c if other else c)}

    own = pl.ds(mo(d * ROWS, ROWS), ROWS)
    loads = []
    for i, (ref, at) in enumerate(((wq, 0), (wk, HEAD), (wv, 2 * HEAD))):
        loads.append(pltpu.make_async_copy(ref, w.at[own, pl.ds(at, HEAD)], load_sem.at[i]))
    loads.append(pltpu.make_async_copy(tok, t.at[0], load_sem.at[3]))
    for copy in loads:
        copy.start()

    barrier = pltpu.get_barrier_semaphore()
    greet = [dev(dx=dx, dy=dy) for dy in range(NY) for dx in range(NX) if dx or dy]
    greet += [dev(dz=1), dev(dz=-1), dev(other=True)]
    for who in greet:
        pl.semaphore_signal(barrier, inc=1, device_id=who, device_id_type=MESH)
    for b in range(NX):
        bias[b] = LOG2E * jnp.concatenate(
            [gate[0:1, (NX * i + b) * TOK : (NX * i + b + 1) * TOK] for i in range(NY)], axis=1)
    pl.semaphore_wait(barrier, len(greet))

    def wrect(zo, row0, rows, col=None, other=False):
        core = 1 - c if other else c
        at = pl.ds(mo((zs(zo) * 2 + core) * ROWS + row0, 16), rows)
        if col is None:
            return w.at[at]
        return w.at[at, pl.ds(col % NY * QKV, QKV)]

    def part(sign):
        return 0 if sign == 1 else HALF

    def seat(n, dy, at=0, count=TOK):
        return qkv.at[n, pl.ds(mo(ys(dy) * TOK + at, 16), count)]

    def regions(name):
        kind, g, sign, i = name
        if kind == "T":
            near = OFF.index(-sign)
            if i == 2:
                at = pl.ds(part(sign), HALF)
                return t.at[near, at], t.at[3, at], t.at[3, at], dev(dx=sign)
            at = pl.ds(part(sign) if i == 0 else part(-sign), HALF)
            return t.at[0, at], t.at[near, at], t.at[near, at], dev(dx=sign)
        if kind == "O":
            source = heads.at[g, pl.ds(mo(ys(sign) * TOK, 16), TOK)]
            return source, out.at[s], out.at[ys(-sign) * NX + xs(-OFF[g])], dev(dx=OFF[g], dy=sign)
        if kind[0] == "E":
            hop = relay.at[i, 0 if sign == 1 else 1]

            def stage(r, at=0, count=TOK):
                return p.at[i, pl.ds(at, count), pl.ds(r * QKV, QKV)]

            if kind == "Er":
                return stage(2, part(sign), HALF), hop, hop, dev(dy=sign)
            if kind == "Ef":
                return (hop, seat(i, -sign, part(sign), HALF), seat(i, -2 * sign, part(sign), HALF),
                        dev(dy=sign))
            return stage(sign % NY), seat(i, 0), seat(i, -sign), dev(dy=sign)
        row0, rows = (0, A_ROWS) if kind[0] == "A" else (A_ROWS, ROWS - A_ROWS)
        half = rows // 2
        if kind[1] == "z":
            col = None if kind == "Az" else 0
            if i == 4:
                row0, rows = row0 + (0 if sign == 1 else half), half
            source = wrect(-sign * (i - 1), row0, rows, col)
            return source, source, wrect(-sign * i, row0, rows, col), dev(dz=sign)
        if kind[1] == "y":
            return wrect(i, row0, rows, 0), wrect(i, row0, rows, -sign), wrect(i, row0, rows, -sign), dev(dy=sign)
        if kind[1] == "f":
            row0, rows = row0 + (0 if sign == 1 else half), half
            return wrect(i, row0, rows, -sign), wrect(i, row0, rows, 2), wrect(i, row0, rows, 2), dev(dy=sign)
        source = wrect(i, row0, rows)
        return source, source, wrect(i, row0, rows, other=True), dev(other=True)

    started, arrived, number = [], set(), {}

    def copy_of(name, source, target, who):
        n = number.setdefault(name, len(number))
        return pltpu.make_async_remote_copy(
            src_ref=source, dst_ref=target, send_sem=send_sem.at[n], recv_sem=recv_sem.at[n],
            device_id=who, device_id_type=MESH)

    def start(name):
        source, target, _, who = regions(name)
        copy_of(name, source, target, who).start()
        started.append(name)

    def arrival(name):
        if name not in arrived:
            arrived.add(name)
            _, _, where, who = regions(name)
            copy_of(name, where, where, who).wait_recv()

    order, messages, work, _, _ = schedule()
    loaded = set()

    def message(name):
        for i in (3,) if name[0] == "T" else (0, 1, 2) if name[0][0] in "AB" else ():
            if i not in loaded:
                loaded.add(i)
                loads[i].wait()
        for need in messages[name][2]:
            if need in messages:
                arrival(need)
        start(name)

    names = [name for name in order if name in work]
    ahead = {}
    waiting = []
    for name in order:
        if name in work:
            ahead[name] = waiting
            waiting = []
        else:
            waiting.append(name)

    def before(name):
        previous = names.index(name) - 1
        if previous >= 0:
            kind, i, j = names[previous]
            if kind == "tile" and j == TILES[-1]:
                for n in BATCHES[i]:
                    qkv[n, pl.ds(mo(y * TOK, TOK), TOK)] = p[n, :, :QKV]
        for item in ahead[name]:
            message(item)
        for need in work[name][1]:
            if need in messages:
                arrival(need)

    def loop(some, run, after=None):
        before(some[0])

        @pl.loop(0, len(some))
        def _(step):
            for k, name in enumerate(some):
                if k:
                    @pl.when(step == k)
                    def _():
                        before(name)
            run(step)
            for k, name in enumerate(some):
                if after and name in after:
                    @pl.when(step == k)
                    def _():
                        after[name]()

    def pick(values, step):
        value = jnp.int32(values[0])
        for k in range(1, len(values)):
            if values[k] != values[k - 1]:
                value = jnp.where(step >= k, values[k], value)
        return value

    for i, batch in enumerate(BATCHES):
        def tile(step):
            j = pick(TILES, step)
            rows = t[batch[0] : batch[-1] + 1].reshape(len(batch) * TOK, D)
            rows = jnp.dot(rows, w[:, pl.ds(mo(j * 256, 256), 256)], preferred_element_type=jnp.float32)
            rows = rows.astype(jnp.bfloat16).reshape(len(batch), TOK, 256)
            for n, block in zip(batch, rows):
                p[n, :, pl.ds(mo(j * 256, 256), 256)] = block

        loop([("tile", i, j) for j in TILES], tile)

    pairs = [name for name in names if name[0] == "pair"]
    local = pltpu.make_async_copy(heads.at[0, pl.ds(mo(y * TOK, 16), TOK)], out.at[s], load_sem.at[4])

    for m in range(NX):
        high[m] = jnp.full((GROUP, HEAD), -1e30, jnp.float32)
        total[m] = jnp.zeros((GROUP, HEAD), jnp.float32)
        summed[m] = jnp.zeros((GROUP, HEAD), jnp.float32)

    def pair(step):
        m, n = pick([name[1] for name in pairs], step), pick([name[2] for name in pairs], step)
        a, b = xs(pick([OFF[name[1]] for name in pairs], step)), xs(pick([OFF[name[2]] for name in pairs], step))
        scale = HEAD**-0.5 * LOG2E
        base, keys = bias[a], bias[b]
        cuts = [(i * TOK, -(-(i + 1) * TOK // HEAD) * HEAD) for i in range(NY)]
        rows = [pl.ds(first, TOK) for first, _ in cuts]
        old = [(high[m, at], total[m, at], summed[m, at]) for at in rows]
        scores = [lax.dot_general(qkv[m, at, :HEAD], qkv[n, :width, HEAD : 2 * HEAD], (((1,), (1,)), ((), ())),
                                  preferred_element_type=jnp.float32) for at, (_, width) in zip(rows, cuts)]
        reach = jnp.clip(lax.broadcasted_iota(jnp.int32, (TOK, HEAD), 0) + (a - b) * TOK, -1, TOK - 1)
        lane = lax.broadcasted_iota(jnp.int32, (TOK, HEAD), 1)
        parts, tops = [], []
        for one, (first, width) in zip(scores, cuts):
            at = -(-first // HEAD) * HEAD
            shift = base[:, at : at + 1] - keys[:, :width]
            some = []
            for at in range(0, width, HEAD):
                part_of = one[:, at : at + HEAD] * scale + shift[:, at : at + HEAD]
                if at + HEAD > first:
                    part_of = jnp.where(lane + (at - first) <= reach, part_of, -1e30)
                some.append(part_of)
            parts.append(some)
            tops.append(jnp.max(fold(some, jnp.maximum), axis=1, keepdims=True))
        new = []
        for some, most, (before_, _, _), (_, width) in zip(parts, tops, old, cuts):
            top = jnp.maximum(before_, most)
            less = jnp.exp2(before_ - top)
            some = [jnp.exp2(one - top) for one in some]
            rounded = jnp.concatenate([one.astype(jnp.bfloat16) for one in some], axis=1)
            value = jnp.dot(rounded, qkv[n, :width, 2 * HEAD :], preferred_element_type=jnp.float32)
            new.append((top, less, fold(some, jnp.add), value))
        for at, (top, less, low, value), (_, total_, summed_) in zip(rows, new, old):
            high[m, at] = top
            total[m, at] = total_ * less + low
            summed[m, at] = summed_ * less + value

    def finish(m):
        heads[m] = (summed[m] / jnp.sum(total[m], axis=1, keepdims=True)).astype(jnp.bfloat16)
        for r in (2, 1, 3, 0):
            if m or r:
                start(("O", m, r, 0))
            else:
                local.start()

    last = {name[1]: name for name in pairs}
    loop(pairs, pair, {name: functools.partial(finish, m) for m, name in last.items()})
    for m in range(NX):
        for r in range(NY):
            if m or r:
                arrival(("O", m, r, 0))
    local.wait()
    for name in started:
        source, target, _, who = regions(name)
        copy_of(name, source, target, who).wait_send()


def merge(heads, out, held, sem):
    come = [pltpu.make_async_copy(heads.at[i], held.at[i], sem.at[0, i]) for i in range(NX * NY)]
    go = [pltpu.make_async_copy(held.at[i], out.at[:, pl.ds(i * HEAD, HEAD)], sem.at[1, i]) for i in range(NX * NY)]
    for copy in come:
        copy.start()
    for one, other in zip(come, go):
        one.wait()
        other.start()
    for copy in go:
        copy.wait()


def body(tokens, query_weight, key_weight, value_weight, cum_gate):
    count = sum(len(m) for m in (weight_messages(), token_messages(), *map(exchange_messages, range(NX))))
    any_space = pl.BlockSpec(memory_space=pl.ANY)
    vmem_space = pl.BlockSpec(memory_space=pltpu.VMEM)
    attended = pl.pallas_call(
        kernel,
        out_shape=jax.ShapeDtypeStruct((NX * NY, TOK, HEAD), jnp.bfloat16),
        in_specs=[any_space] * 4 + [vmem_space],
        out_specs=any_space,
        scratch_shapes=[
            pltpu.VMEM((D, NY * 3 * HEAD), jnp.bfloat16),
            pltpu.VMEM((NX, TOK, D), jnp.bfloat16),
            pltpu.VMEM((NX, TOK, NY * QKV), jnp.bfloat16),
            pltpu.VMEM((NX, 2, HALF, QKV), jnp.bfloat16),
            pltpu.VMEM((NX, GROUP, QKV), jnp.bfloat16),
            pltpu.VMEM((NX, 1, GROUP), jnp.float32),
            pltpu.VMEM((NX, GROUP, HEAD), jnp.float32),
            pltpu.VMEM((NX, GROUP, HEAD), jnp.float32),
            pltpu.VMEM((NX, GROUP, HEAD), jnp.float32),
            pltpu.VMEM((NX, GROUP, HEAD), jnp.bfloat16),
            pltpu.SemaphoreType.DMA((5,)),
            pltpu.SemaphoreType.DMA((count + NX * NY,)),
            pltpu.SemaphoreType.DMA((count + NX * NY,)),
        ],
        compiler_params=pltpu.CompilerParams(
            collective_id=0, has_side_effects=True, vmem_limit_bytes=60 * 1024 * 1024
        ),
        name="mixer",
    )(tokens[0], query_weight, key_weight, value_weight, cum_gate[0])
    merged = pl.pallas_call(
        merge,
        out_shape=jax.ShapeDtypeStruct((TOK, NX * NY * HEAD), jnp.bfloat16),
        in_specs=[any_space],
        out_specs=any_space,
        scratch_shapes=[pltpu.VMEM((NX * NY, TOK, HEAD), jnp.bfloat16), pltpu.SemaphoreType.DMA((2, NX * NY))],
        name="merge",
    )(attended)
    return merged[None]


def solution(mesh):
    in_specs = (
        P("dp", "sp", None),
        P("dp", "sp"),
        P("dp", "sp"),
        P("dp", "sp"),
        P("dp", "sp", None),
    )
    out_specs = P("dp", "sp", None)
    return jax.shard_map(body, mesh=mesh, in_specs=in_specs, out_specs=out_specs, check_vma=False)
```

time: 273 us -> 101 us (0.37)
  waiting for transfers between devices: 203 us -> 0 us
  Pallas kernels: 0 us -> 101 us
  matrix products: 28 us -> 0 us
  blocking collectives: 18.2 us -> 0 us
  between operations: 13.5 us -> 0.01 us
  other arithmetic: 5.45 us -> 0 us
  local copies, waits for them, and re-layouts: 3.96 us -> 0 us
    all_gather x2 -> x0, waiting for transfers between devices: 202 us -> none  [the longest x1 160 us: body(): lax.all_gather(own_rows, 'sp', axis=0, tiled=True)]
    pallas_call x0 -> x2, Pallas kernels: none -> 101 us  [the longest x1 98.7 us: body(): pl.pallas_call(kernel, out_shape=jax.ShapeDtypeStruct((NX * NY, TOK, HEAD...]
    dot_general x13 -> x0, matrix products: 28 us -> none  [the longest x1 16 us: body(): jnp.dot(lax.all_gather(own_rows, 'sp', axis=0, tiled=True), stacked, pref...]
    all_to_all x1 -> x0, blocking collectives: 18.2 us -> none  [body(): lax.all_to_all(head_out, 'sp', split_axis=0, concat_axis=1, tiled=True)]
    reduce_sum x6 -> x0, other arithmetic: 3.83 us -> none  [attend(): total = jnp.sum(weights, axis=1, keepdims=True)]
  transfers between devices with their start and end apart: 2 -> 0, of which waited for: 2 -> 0; matrix products, arithmetic and copies ran while one was open for 1% -> 0% of each run, Pallas kernels for 0% -> 0%
where the time goes in v4:
time: 101 us
  Pallas kernels  101 us (100%)
    pallas_call x1, Pallas kernels, body(): pl.pallas_call(kernel, out_shape=jax.ShapeDtypeStruct((NX * NY, TOK, HEAD...  98.7 us
    pallas_call x1, Pallas kernels, body(): pl.pallas_call(merge, out_shape=jax.ShapeDtypeStruct((TOK, NX * NY * HEAD...  2.03 us

profile of v4, /device:TPU:1, one launch (start us, length us, event | category | flops | bytes accessed | tf_op | source)
XLA Modules:
  0.0 100.7 jit_solution(18336670973917523466)
XLA Ops:
  0.0 98.7 %mixer.1.heads = bf16[16,192,128]{2,1,0:T(8,128)(2,1)} custom-call(bf16[192,4096]{1,0:T(8,128)(2,1)} %bitcast.3, bf16[256,128]{1,0:T(8,128)(2,1)} %wq.1, bf16[256,128]{1,0:T(8,128)(2,1)} %wk.1, bf16[256,128]{1,0:T(8,128)(2,1)} %wv.1, f32[1,3072]{1,0:T(1,128)} %bitcast.4), custom_call_target="tpu_custom_call" | custom-call | tf_op jit(solution)/shard_map/mixer/pallas_call | solution.py:403
  98.7 2.0 %merge.1 = bf16[192,2048]{1,0:T(8,128)(2,1)} custom-call(bf16[16,192,128]{2,1,0:T(8,128)(2,1)} %mixer.1.heads), custom_call_target="tpu_custom_call" | custom-call | tf_op jit(solution)/shard_map/merge/pallas_call | solution.py:428

commit v5 on v4

--- a/solution.py
+++ b/solution.py
@@ -20,8 +20,12 @@
 A_ROWS = 96
 ORDER = (0, -1, 1, -2, 2, -3, 3, 4)
 OFF = (0, -1, 1, 2)
-BATCHES = ((0, 1, 2), (3,))
-TILE_US, PAIR_US = (1.4, 0.65), 0.9
+BATCHES = ((0,), (1, 2), (3,))
+TILE_US, PAIR_US = (0.65, 1.05, 0.65), 1.75
+PAIRS = (((0, 0), (1, 1)), ((0, 1), (1, 0)), ((2, 2), (1, 2)), ((2, 0), (2, 1)),
+         ((3, 3), (1, 3)), ((3, 0), (2, 3)), ((3, 1), (3, 2)), ((0, 2), (0, 3)))
+DONE = {4: (1,), 5: (2,), 6: (3,), 7: (0,)}
+SPLIT = tuple((m, r) for m in (3, 1, 2, 0) for r in range(NY) if m == 3 or r == 2)
 TILES = (3, 4, 5, 2, 1, 0)
 
 
@@ -91,11 +95,8 @@
             need = [k for n in batch for k in tokens[n]] + list(weight_messages())
             t["tile", i, j] = (TILE_US[i], need)
     done = [[(kind, 0, sign, n) for kind in ("Ey", "Ef") for sign in (1, -1)] for n in range(NX)]
-    last = NX - 1
-    order = [(m, n) for m in range(last) for n in range(last)]
-    order += [(last, n) for n in range(NX)] + [(m, last) for m in (1, 2, 0)]
-    for m, n in order:
-        t["pair", m, n] = (PAIR_US, done[n] + done[m])
+    for k, some in enumerate(PAIRS):
+        t["pair", k, 0] = (PAIR_US, [one for mn in some for i in mn for one in done[i]])
     names = list(t)
     for before, name in zip(names, names[1:]):
         t[name][1].append(before)
@@ -140,7 +141,7 @@
     return functools.reduce(op, parts)
 
 
-def kernel(tok, wq, wk, wv, gate, out, w, t, p, relay, qkv, bias, high, total, summed, heads,
+def kernel(tok, wq, wk, wv, gate, out, w, t, p, relay, qkv, bias, high, total, summed, heads, relay_out,
            load_sem, send_sem, recv_sem):
     s, d = lax.axis_index("sp"), lax.axis_index("dp")
     y, x = lax.div(s, NX), lax.rem(s, NX)
@@ -199,8 +200,18 @@
             at = pl.ds(part(sign) if i == 0 else part(-sign), HALF)
             return t.at[0, at], t.at[near, at], t.at[near, at], dev(dx=sign)
         if kind == "O":
-            source = heads.at[g, pl.ds(mo(ys(sign) * TOK, 16), TOK)]
-            return source, out.at[s], out.at[ys(-sign) * NX + xs(-OFF[g])], dev(dx=OFF[g], dy=sign)
+            count = HALF if (g, sign) in SPLIT else TOK
+            source = heads.at[g, pl.ds(mo(ys(sign) * TOK, 16), count)]
+            rows = pl.ds(0, count)
+            return source, out.at[s, rows], out.at[ys(-sign) * NX + xs(-OFF[g]), rows], dev(dx=OFF[g], dy=sign)
+        if kind in ("R", "F"):
+            hop = relay_out.at[SPLIT.index((g, sign))]
+            near = (-1 if g == 3 else OFF[g], -1 if sign == 2 else sign)
+            if kind == "R":
+                return heads.at[g, pl.ds(mo(ys(sign) * TOK + HALF, 16), HALF)], hop, hop, dev(*near)
+            rows = pl.ds(HALF, HALF)
+            return (hop, out.at[ys(-near[1]) * NX + xs(-near[0]), rows],
+                    out.at[ys(-sign) * NX + xs(-OFF[g]), rows], dev(-1 if g == 3 else 0, -1 if sign == 2 else 0))
         if kind[0] == "E":
             hop = relay.at[i, 0 if sign == 1 else 1]
 
@@ -280,6 +291,11 @@
                     qkv[n, pl.ds(mo(y * TOK, TOK), TOK)] = p[n, :, :QKV]
         for item in ahead[name]:
             message(item)
+        if name == names[-1]:
+            for m, r in SPLIT:
+                if m in (1, 2):
+                    arrival(("R", m, r, 0))
+                    start(("F", m, r, 0))
         for need in work[name][1]:
             if need in messages:
                 arrival(need)
@@ -327,9 +343,9 @@
         total[m] = jnp.zeros((GROUP, HEAD), jnp.float32)
         summed[m] = jnp.zeros((GROUP, HEAD), jnp.float32)
 
-    def pair(step):
-        m, n = pick([name[1] for name in pairs], step), pick([name[2] for name in pairs], step)
-        a, b = xs(pick([OFF[name[1]] for name in pairs], step)), xs(pick([OFF[name[2]] for name in pairs], step))
+    def pair(step, which):
+        m, n = (pick([some[which][i] for some in PAIRS], step) for i in (0, 1))
+        a, b = (xs(pick([OFF[some[which][i]] for some in PAIRS], step)) for i in (0, 1))
         scale = HEAD**-0.5 * LOG2E
         base, keys = bias[a], bias[b]
         cuts = [(i * TOK, -(-(i + 1) * TOK // HEAD) * HEAD) for i in range(NY)]
@@ -367,17 +383,29 @@
     def finish(m):
         heads[m] = (summed[m] / jnp.sum(total[m], axis=1, keepdims=True)).astype(jnp.bfloat16)
         for r in (2, 1, 3, 0):
+            if (m, r) in SPLIT:
+                start(("R", m, r, 0))
+        for r in (2, 1, 3, 0):
             if m or r:
                 start(("O", m, r, 0))
             else:
                 local.start()
 
-    last = {name[1]: name for name in pairs}
-    loop(pairs, pair, {name: functools.partial(finish, m) for m, name in last.items()})
+    def run(step):
+        pair(step, 0)
+        pair(step, 1)
+
+    loop(pairs, run, {pairs[k]: functools.partial(lambda ms: [finish(m) for m in ms], ms) for k, ms in DONE.items()})
+    for m, r in SPLIT:
+        if m in (0, 3):
+            arrival(("R", m, r, 0))
+            start(("F", m, r, 0))
     for m in range(NX):
         for r in range(NY):
             if m or r:
                 arrival(("O", m, r, 0))
+    for m, r in SPLIT:
+        arrival(("F", m, r, 0))
     local.wait()
     for name in started:
         source, target, _, who = regions(name)
@@ -416,9 +444,10 @@
             pltpu.VMEM((NX, GROUP, HEAD), jnp.float32),
             pltpu.VMEM((NX, GROUP, HEAD), jnp.float32),
             pltpu.VMEM((NX, GROUP, HEAD), jnp.bfloat16),
+            pltpu.VMEM((len(SPLIT), HALF, HEAD), jnp.bfloat16),
             pltpu.SemaphoreType.DMA((5,)),
-            pltpu.SemaphoreType.DMA((count + NX * NY,)),
-            pltpu.SemaphoreType.DMA((count + NX * NY,)),
+            pltpu.SemaphoreType.DMA((count + NX * NY + 2 * len(SPLIT),)),
+            pltpu.SemaphoreType.DMA((count + NX * NY + 2 * len(SPLIT),)),
         ],
         compiler_params=pltpu.CompilerParams(
             collective_id=0, has_side_effects=True, vmem_limit_bytes=60 * 1024 * 1024

time: 101 us -> 98.7 us (0.977)
  Pallas kernels: 101 us -> 98.3 us
    pallas_call x1, Pallas kernels: 98.7 us -> 96.2 us  [body(): pl.pallas_call(kernel, out_shape=jax.ShapeDtypeStruct((NX * NY, TOK, HEAD...]
where the time goes in v5:
time: 98.7 us; the launch traced here: 98.3 us
  Pallas kernels  98.3 us (100%)
    pallas_call x1, Pallas kernels, body(): pl.pallas_call(kernel, out_shape=jax.ShapeDtypeStruct((NX * NY, TOK, HEAD...  96.2 us
    pallas_call x1, Pallas kernels, body(): pl.pallas_call(merge, out_shape=jax.ShapeDtypeStruct((TOK, NX * NY * HEAD...  2.03 us

profile of v5, /device:TPU:1, one launch (start us, length us, event | category | flops | bytes accessed | tf_op | source)
XLA Modules:
  0.0 98.3 jit_solution(3760475848440733635)
XLA Ops:
  0.0 96.2 %mixer.1.heads = bf16[16,192,128]{2,1,0:T(8,128)(2,1)} custom-call(bf16[192,4096]{1,0:T(8,128)(2,1)} %bitcast.3, bf16[256,128]{1,0:T(8,128)(2,1)} %wq.1, bf16[256,128]{1,0:T(8,128)(2,1)} %wk.1, bf16[256,128]{1,0:T(8,128)(2,1)} %wv.1, f32[1,3072]{1,0:T(1,128)} %bitcast.4), custom_call_target="tpu_custom_call" | custom-call | tf_op jit(solution)/shard_map/mixer/pallas_call | solution.py:431
  96.3 2.0 %merge.1 = bf16[192,2048]{1,0:T(8,128)(2,1)} custom-call(bf16[16,192,128]{2,1,0:T(8,128)(2,1)} %mixer.1.heads), custom_call_target="tpu_custom_call" | custom-call | tf_op jit(solution)/shard_map/merge/pallas_call | solution.py:457

commit v6 on v5

--- a/solution.py
+++ b/solution.py
@@ -16,12 +16,15 @@
 GROUP = NY * TOK
 LOG2E = 1.4426950408889634
 
+WIDE = (2 * HEAD, HEAD)
+FIRST = (0, NY * 2 * HEAD)
 QKV = 3 * HEAD
-A_ROWS = 96
+A_ROWS = (64, 224)
 ORDER = (0, -1, 1, -2, 2, -3, 3, 4)
 OFF = (0, -1, 1, 2)
-BATCHES = ((0,), (1, 2), (3,))
-TILE_US, PAIR_US = (0.65, 1.05, 0.65), 1.75
+LOOPS = (((0,), (2, 3, 1, 0), 0.65), ((1, 2), (2, 3, 1, 0), 1.05), ((0, 1, 2), (5, 4), 1.4), ((3,), (2, 3, 1, 0, 5, 4), 0.65))
+PAIR_US = 1.75
+RELAY_US = 4.0
 PAIRS = (((0, 0), (1, 1)), ((0, 1), (1, 0)), ((2, 2), (1, 2)), ((2, 0), (2, 1)),
          ((3, 3), (1, 3)), ((3, 0), (2, 3)), ((3, 1), (3, 2)), ((0, 2), (0, 3)))
 DONE = {4: (1,), 5: (2,), 6: (3,), 7: (0,)}
@@ -29,8 +32,8 @@
 TILES = (3, 4, 5, 2, 1, 0)
 
 
-def weight_messages():
-    a, b, g = A_ROWS * QKV * 2, (ROWS - A_ROWS) * QKV * 2, 0
+def weight_messages(g):
+    a, b = A_ROWS[g] * WIDE[g] * 2, (ROWS - A_ROWS[g]) * WIDE[g] * 2
     m = {}
     for sign, link in ((1, "y+"), (-1, "y-")):
         m["Ay", g, sign, 0] = (link, a, [])
@@ -73,30 +76,31 @@
     return m
 
 
-def batch_of(n):
-    return next(i for i, batch in enumerate(BATCHES) if n in batch)
+def tile_of(n, j):
+    return next(("tile", i, j) for i, (blocks, tiles, _) in enumerate(LOOPS) if n in blocks and j in tiles)
 
 
 def exchange_messages(n):
     m = {}
-    size = TOK * QKV * 2
-    for sign, link in ((1, "y+"), (-1, "y-")):
-        m["Er", 0, sign, n] = (link, size / 2, [("tile", batch_of(n), 3), ("tile", batch_of(n), 4)])
-        m["Ef", 0, sign, n] = (link, size / 2, [("Er", 0, sign, n)])
-        m["Ey", 0, sign, n] = (link, size, [("tile", batch_of(n), 5 if sign < 0 else 1)])
+    for g in (0, 1):
+        size = TOK * WIDE[g] * 2
+        tile = [tile_of(n, r if g == 0 else 4 + r // 2) for r in range(NY)]
+        for sign, link in ((1, "y+"), (-1, "y-")):
+            m["Er", g, sign, n] = (link, size / 2, [tile[2]])
+            m["Ef", g, sign, n] = (link, size / 2, [("Er", g, sign, n)])
+            m["Ey", g, sign, n] = (link, size, [tile[sign % NY]])
     return m
 
 
 def tasks():
     t = {}
     tokens = ([], [("T", 0, 1, 0), ("T", 0, 1, 1)], [("T", 0, -1, 0), ("T", 0, -1, 1)], [("T", 0, 1, 2), ("T", 0, -1, 2)])
-    for i, batch in enumerate(BATCHES):
-        for j in TILES:
-            need = [k for n in batch for k in tokens[n]] + list(weight_messages())
-            t["tile", i, j] = (TILE_US[i], need)
-    done = [[(kind, 0, sign, n) for kind in ("Ey", "Ef") for sign in (1, -1)] for n in range(NX)]
+    for i, (blocks, tiles, time) in enumerate(LOOPS):
+        for j in tiles:
+            t["tile", i, j] = (time, [k for n in blocks for k in tokens[n]] + list(weight_messages(j // 4)))
+    done = [[[(kind, g, sign, n) for kind in ("Ey", "Ef") for sign in (1, -1)] for n in range(NX)] for g in (0, 1)]
     for k, some in enumerate(PAIRS):
-        t["pair", k, 0] = (PAIR_US, [one for mn in some for i in mn for one in done[i]])
+        t["pair", k, 0] = (PAIR_US, [one for q, k_ in some for one in done[1][q] + done[0][k_]])
     names = list(t)
     for before, name in zip(names, names[1:]):
         t[name][1].append(before)
@@ -105,7 +109,7 @@
 
 def schedule():
     messages = {}
-    for some in (weight_messages(), token_messages(), *(exchange_messages(n) for n in range(NX))):
+    for some in (weight_messages(0), token_messages(), weight_messages(1), *(exchange_messages(n) for n in range(NX))):
         messages.update(some)
     work = tasks()
     place = {name: i for i, name in enumerate([*messages, *work])}
@@ -129,7 +133,7 @@
             link, size, _ = messages[name]
             end = max(now, free.get(link, 0.0)) + (size / 600e3 if link == "d" else size / 45e3)
             free[link] = end
-            done[name] = end + (1.0 if link == "d" else 1.8)
+            done[name] = end + (1.0 if link == "d" else RELAY_US if name[0] == "Er" and name[3] < 3 else 1.8)
     return order, messages, work, done, free
 
 
@@ -141,7 +145,7 @@
     return functools.reduce(op, parts)
 
 
-def kernel(tok, wq, wk, wv, gate, out, w, t, p, relay, qkv, bias, high, total, summed, heads, relay_out,
+def kernel(tok, wq, wk, wv, gate, out, w, t, p, relay_kv, relay_q, kv, qs, bias, high, total, summed, heads, relay_out,
            load_sem, send_sem, recv_sem):
     s, d = lax.axis_index("sp"), lax.axis_index("dp")
     y, x = lax.div(s, NX), lax.rem(s, NX)
@@ -161,7 +165,7 @@
 
     own = pl.ds(mo(d * ROWS, ROWS), ROWS)
     loads = []
-    for i, (ref, at) in enumerate(((wq, 0), (wk, HEAD), (wv, 2 * HEAD))):
+    for i, (ref, at) in enumerate(((wk, 0), (wv, HEAD), (wq, FIRST[1]))):
         loads.append(pltpu.make_async_copy(ref, w.at[own, pl.ds(at, HEAD)], load_sem.at[i]))
     loads.append(pltpu.make_async_copy(tok, t.at[0], load_sem.at[3]))
     for copy in loads:
@@ -177,18 +181,18 @@
             [gate[0:1, (NX * i + b) * TOK : (NX * i + b + 1) * TOK] for i in range(NY)], axis=1)
     pl.semaphore_wait(barrier, len(greet))
 
-    def wrect(zo, row0, rows, col=None, other=False):
+    def wrect(g, zo, row0, rows, col=None, other=False):
         core = 1 - c if other else c
         at = pl.ds(mo((zs(zo) * 2 + core) * ROWS + row0, 16), rows)
         if col is None:
-            return w.at[at]
-        return w.at[at, pl.ds(col % NY * QKV, QKV)]
+            return w.at[at, pl.ds(FIRST[g], NY * WIDE[g])]
+        return w.at[at, pl.ds(FIRST[g] + col % NY * WIDE[g], WIDE[g])]
 
     def part(sign):
         return 0 if sign == 1 else HALF
 
-    def seat(n, dy, at=0, count=TOK):
-        return qkv.at[n, pl.ds(mo(ys(dy) * TOK + at, 16), count)]
+    def seat(g, n, dy, at=0, count=TOK):
+        return (kv, qs)[g].at[n, pl.ds(mo(ys(dy) * TOK + at, 16), count)]
 
     def regions(name):
         kind, g, sign, i = name
@@ -213,32 +217,34 @@
             return (hop, out.at[ys(-near[1]) * NX + xs(-near[0]), rows],
                     out.at[ys(-sign) * NX + xs(-OFF[g]), rows], dev(-1 if g == 3 else 0, -1 if sign == 2 else 0))
         if kind[0] == "E":
-            hop = relay.at[i, 0 if sign == 1 else 1]
+            hop = (relay_kv, relay_q)[g].at[i, 0 if sign == 1 else 1]
 
             def stage(r, at=0, count=TOK):
-                return p.at[i, pl.ds(at, count), pl.ds(r * QKV, QKV)]
+                if g == 0:
+                    return p.at[i, r, pl.ds(at, count)]
+                return p.at[i, 4 + r // 2, pl.ds(at, count), pl.ds(r % 2 * HEAD, HEAD)]
 
             if kind == "Er":
                 return stage(2, part(sign), HALF), hop, hop, dev(dy=sign)
             if kind == "Ef":
-                return (hop, seat(i, -sign, part(sign), HALF), seat(i, -2 * sign, part(sign), HALF),
+                return (hop, seat(g, i, -sign, part(sign), HALF), seat(g, i, -2 * sign, part(sign), HALF),
                         dev(dy=sign))
-            return stage(sign % NY), seat(i, 0), seat(i, -sign), dev(dy=sign)
-        row0, rows = (0, A_ROWS) if kind[0] == "A" else (A_ROWS, ROWS - A_ROWS)
+            return stage(sign % NY), seat(g, i, 0), seat(g, i, -sign), dev(dy=sign)
+        row0, rows = (0, A_ROWS[g]) if kind[0] == "A" else (A_ROWS[g], ROWS - A_ROWS[g])
         half = rows // 2
         if kind[1] == "z":
             col = None if kind == "Az" else 0
             if i == 4:
                 row0, rows = row0 + (0 if sign == 1 else half), half
-            source = wrect(-sign * (i - 1), row0, rows, col)
-            return source, source, wrect(-sign * i, row0, rows, col), dev(dz=sign)
+            source = wrect(g, -sign * (i - 1), row0, rows, col)
+            return source, source, wrect(g, -sign * i, row0, rows, col), dev(dz=sign)
         if kind[1] == "y":
-            return wrect(i, row0, rows, 0), wrect(i, row0, rows, -sign), wrect(i, row0, rows, -sign), dev(dy=sign)
+            return wrect(g, i, row0, rows, 0), wrect(g, i, row0, rows, -sign), wrect(g, i, row0, rows, -sign), dev(dy=sign)
         if kind[1] == "f":
             row0, rows = row0 + (0 if sign == 1 else half), half
-            return wrect(i, row0, rows, -sign), wrect(i, row0, rows, 2), wrect(i, row0, rows, 2), dev(dy=sign)
-        source = wrect(i, row0, rows)
-        return source, source, wrect(i, row0, rows, other=True), dev(other=True)
+            return wrect(g, i, row0, rows, -sign), wrect(g, i, row0, rows, 2), wrect(g, i, row0, rows, 2), dev(dy=sign)
+        source = wrect(g, i, row0, rows)
+        return source, source, wrect(g, i, row0, rows, other=True), dev(other=True)
 
     started, arrived, number = [], set(), {}
 
@@ -286,14 +292,18 @@
         previous = names.index(name) - 1
         if previous >= 0:
             kind, i, j = names[previous]
-            if kind == "tile" and j == TILES[-1]:
-                for n in BATCHES[i]:
-                    qkv[n, pl.ds(mo(y * TOK, TOK), TOK)] = p[n, :, :QKV]
+            if kind == "tile" and j in (0, 4):
+                for n in LOOPS[i][0]:
+                    at = pl.ds(mo(y * TOK, TOK), TOK)
+                    if j == 0:
+                        kv[n, at] = p[n, 0]
+                    else:
+                        qs[n, at] = p[n, 4, :, :HEAD]
         for item in ahead[name]:
             message(item)
         if name == names[-1]:
             for m, r in SPLIT:
-                if m in (1, 2):
+                if m == 1:
                     arrival(("R", m, r, 0))
                     start(("F", m, r, 0))
         for need in work[name][1]:
@@ -324,16 +334,16 @@
                 value = jnp.where(step >= k, values[k], value)
         return value
 
-    for i, batch in enumerate(BATCHES):
+    for i, (blocks, tiles, _) in enumerate(LOOPS):
         def tile(step):
-            j = pick(TILES, step)
-            rows = t[batch[0] : batch[-1] + 1].reshape(len(batch) * TOK, D)
+            j = pick(tiles, step)
+            rows = t[blocks[0] : blocks[-1] + 1].reshape(len(blocks) * TOK, D)
             rows = jnp.dot(rows, w[:, pl.ds(mo(j * 256, 256), 256)], preferred_element_type=jnp.float32)
-            rows = rows.astype(jnp.bfloat16).reshape(len(batch), TOK, 256)
-            for n, block in zip(batch, rows):
-                p[n, :, pl.ds(mo(j * 256, 256), 256)] = block
-
-        loop([("tile", i, j) for j in TILES], tile)
+            rows = rows.astype(jnp.bfloat16).reshape(len(blocks), TOK, 256)
+            for n, block in zip(blocks, rows):
+                p[n, j] = block
+
+        loop([("tile", i, j) for j in tiles], tile)
 
     pairs = [name for name in names if name[0] == "pair"]
     local = pltpu.make_async_copy(heads.at[0, pl.ds(mo(y * TOK, 16), TOK)], out.at[s], load_sem.at[4])
@@ -351,7 +361,7 @@
         cuts = [(i * TOK, -(-(i + 1) * TOK // HEAD) * HEAD) for i in range(NY)]
         rows = [pl.ds(first, TOK) for first, _ in cuts]
         old = [(high[m, at], total[m, at], summed[m, at]) for at in rows]
-        scores = [lax.dot_general(qkv[m, at, :HEAD], qkv[n, :width, HEAD : 2 * HEAD], (((1,), (1,)), ((), ())),
+        scores = [lax.dot_general(qs[m, at], kv[n, :width, :HEAD], (((1,), (1,)), ((), ())),
                                   preferred_element_type=jnp.float32) for at, (_, width) in zip(rows, cuts)]
         reach = jnp.clip(lax.broadcasted_iota(jnp.int32, (TOK, HEAD), 0) + (a - b) * TOK, -1, TOK - 1)
         lane = lax.broadcasted_iota(jnp.int32, (TOK, HEAD), 1)
@@ -373,7 +383,7 @@
             less = jnp.exp2(before_ - top)
             some = [jnp.exp2(one - top) for one in some]
             rounded = jnp.concatenate([one.astype(jnp.bfloat16) for one in some], axis=1)
-            value = jnp.dot(rounded, qkv[n, :width, 2 * HEAD :], preferred_element_type=jnp.float32)
+            value = jnp.dot(rounded, kv[n, :width, HEAD:], preferred_element_type=jnp.float32)
             new.append((top, less, fold(some, jnp.add), value))
         for at, (top, less, low, value), (_, total_, summed_) in zip(rows, new, old):
             high[m, at] = top
@@ -397,7 +407,7 @@
 
     loop(pairs, run, {pairs[k]: functools.partial(lambda ms: [finish(m) for m in ms], ms) for k, ms in DONE.items()})
     for m, r in SPLIT:
-        if m in (0, 3):
+        if m != 1:
             arrival(("R", m, r, 0))
             start(("F", m, r, 0))
     for m in range(NX):
@@ -425,7 +435,7 @@
 
 
 def body(tokens, query_weight, key_weight, value_weight, cum_gate):
-    count = sum(len(m) for m in (weight_messages(), token_messages(), *map(exchange_messages, range(NX))))
+    count = sum(len(m) for m in (weight_messages(0), weight_messages(1), token_messages(), *map(exchange_messages, range(NX))))
     any_space = pl.BlockSpec(memory_space=pl.ANY)
     vmem_space = pl.BlockSpec(memory_space=pltpu.VMEM)
     attended = pl.pallas_call(
@@ -436,9 +446,11 @@
         scratch_shapes=[
             pltpu.VMEM((D, NY * 3 * HEAD), jnp.bfloat16),
             pltpu.VMEM((NX, TOK, D), jnp.bfloat16),
-            pltpu.VMEM((NX, TOK, NY * QKV), jnp.bfloat16),
-            pltpu.VMEM((NX, 2, HALF, QKV), jnp.bfloat16),
-            pltpu.VMEM((NX, GROUP, QKV), jnp.bfloat16),
+            pltpu.VMEM((NX, 6, TOK, 2 * HEAD), jnp.bfloat16),
+            pltpu.VMEM((NX, 2, HALF, 2 * HEAD), jnp.bfloat16),
+            pltpu.VMEM((NX, 2, HALF, HEAD), jnp.bfloat16),
+            pltpu.VMEM((NX, GROUP, 2 * HEAD), jnp.bfloat16),
+            pltpu.VMEM((NX, GROUP, HEAD), jnp.bfloat16),
             pltpu.VMEM((NX, 1, GROUP), jnp.float32),
             pltpu.VMEM((NX, GROUP, HEAD), jnp.float32),
             pltpu.VMEM((NX, GROUP, HEAD), jnp.float32),

time: 98.7 us -> 96.9 us (0.982)
  Pallas kernels: 98.3 us -> 96.7 us
    pallas_call x1, Pallas kernels: 96.2 us -> 94.7 us  [body(): pl.pallas_call(kernel, out_shape=jax.ShapeDtypeStruct((NX * NY, TOK, HEAD...]
where the time goes in v6:
time: 96.9 us; the launch traced here: 96.7 us
  Pallas kernels  96.7 us (100%)
    pallas_call x1, Pallas kernels, body(): pl.pallas_call(kernel, out_shape=jax.ShapeDtypeStruct((NX * NY, TOK, HEAD...  94.7 us
    pallas_call x1, Pallas kernels, body(): pl.pallas_call(merge, out_shape=jax.ShapeDtypeStruct((TOK, NX * NY * HEAD...  2.03 us

profile of v6, /device:TPU:1, one launch (start us, length us, event | category | flops | bytes accessed | tf_op | source)
XLA Modules:
  0.0 96.7 jit_solution(3368555145915164410)
XLA Ops:
  0.0 94.7 %mixer.1.heads = bf16[16,192,128]{2,1,0:T(8,128)(2,1)} custom-call(bf16[192,4096]{1,0:T(8,128)(2,1)} %bitcast.3, bf16[256,128]{1,0:T(8,128)(2,1)} %wq.1, bf16[256,128]{1,0:T(8,128)(2,1)} %wk.1, bf16[256,128]{1,0:T(8,128)(2,1)} %wv.1, f32[1,3072]{1,0:T(1,128)} %bitcast.4), custom_call_target="tpu_custom_call" | custom-call | tf_op jit(solution)/shard_map/mixer/pallas_call | solution.py:441
  94.7 2.0 %merge.1 = bf16[192,2048]{1,0:T(8,128)(2,1)} custom-call(bf16[16,192,128]{2,1,0:T(8,128)(2,1)} %mixer.1.heads), custom_call_target="tpu_custom_call" | custom-call | tf_op jit(solution)/shard_map/merge/pallas_call | solution.py:469
